TPU v7x, 256 devices: a whole 4x4x8 slice. The times are simulated.
256 devices in a mesh: sp: 16 (over y, x), tp: 16 (over z, core).
Axes of the slice: x: 4, y: 4, z: 8, core: 2. Of those that a mesh axis runs over, the one named last changes fastest.
Arguments:
- receptance: bfloat16 [4096, 1024], P('sp', 'tp'), may hold values from -6 to 6
- key_matrix: bfloat16 [4096, 1024], P('sp', 'tp'), may hold values from -6 to 6
- value_matrix: bfloat16 [4096, 1024], P('sp', 'tp'), may hold values from -6 to 6
- decay_input_term: bfloat16 [4096, 1024], P('sp', 'tp'), may hold values from -5 to 5
- decay_channel_offset: float32 [1024], P('tp'), may hold values from -12 to -2
- head_log_decay: float32 [4096, 16], P('sp', 'tp'), may hold values from -2 to 0
- context_step_logits: bfloat16 [4096, 1024], P('sp', 'tp'), may hold values from -16 to 4
- head_gate_rows: bfloat16 [4096, 1024], P('sp', 'tp'), may hold values from -6 to 6
- head_norm_scale: float32 [1024], P('tp'), may hold values from 0.1 to 1.9
- mixer_output_weight: bfloat16 [1024, 2048], replicated, may hold values from -0.1875 to 0.1875
- residual: bfloat16 [4096, 2048], P(('sp', 'tp')), may hold values from -6 to 6
- expert_norm_scale: float32 [2048], replicated, may hold values from 0.1 to 1.9
- expert_index_table: int32 [4096, 2], P(('sp', 'tp')), may hold values from 0 to 15, all different within a row; in each aligned block of 16 rows (0 to 15, 16 to 31, ...) at most 4 rows name the same one
- expert_router_scores: float32 [4096, 2], P(('sp', 'tp')), may hold values from -6 to 6
- expert_gate_weight: bfloat16 [16, 2048, 7168], P('sp', None, 'tp'), may hold values from -0.125 to 0.125
- expert_up_weight: bfloat16 [16, 2048, 7168], P('sp', None, 'tp'), may hold values from -0.125 to 0.125
- expert_down_weight: bfloat16 [16, 7168, 2048], P('sp', 'tp'), may hold values from -0.0625 to 0.0625
Outputs:
- layer_out: bfloat16 [4096, 2048], P(('sp', 'tp'))
Inputs may be any that keep to these rules, and one draw needn't show every extreme that they name: `expert_index_table`: each row names 2 different experts. In each aligned block of 16 rows no expert is named more than 4 times, a bound that some block reaches.
All inputs are finite; a program needn't handle non-finite values.
Results may differ from a plain program's by a relative error of at most 0.018.
Values may be sent and summed in bfloat16 or wider, within the bound.
A program may use at most 64 MiB of HBM per device.

v0:
```python
import jax
import jax.numpy as jnp
from jax import lax
from jax.sharding import PartitionSpec as P

HEAD_CHANNELS = 64
TOPK = 2


decay_factor = 0.6065306597126334
group_eps = 0.00064
norm_eps = 1e-06
key_eps = 1e-06
highest = lax.Precision.HIGHEST
block_len = 64
run_len = 8


def copy_for_each(shard, axis):
    copies = jnp.broadcast_to(shard, (lax.axis_size(axis), *shard.shape))
    return lax.all_to_all(copies, axis, split_axis=0, concat_axis=0, tiled=True)


def all_in_one(shard, axis):
    leaves = jax.tree.leaves(shard)
    order = sorted(range(len(leaves)), key=lambda k: -leaves[k].size)
    width = (1, *leaves[order[0]].shape)[-1]
    lines = [
        jnp.pad(leaves[k].reshape(-1), (0, -leaves[k].size % width)).reshape(-1, width)
        for k in order
    ]
    both, at, found = (copy_for_each(jnp.concatenate(lines), axis), 0, {})
    for k, line in zip(order, lines):
        share = both[:, at : at + len(line)].reshape(len(both), -1)
        found[k] = share[:, : leaves[k].size].reshape(-1, *leaves[k].shape)
        at += len(line)
    numbers = iter(range(len(leaves)))
    return jax.tree.map(lambda _: found[next(numbers)], shard)


def folded_in_pairs(pieces, combine):
    while len(jax.tree.leaves(pieces)[0]) > 1:
        pieces = jax.vmap(combine)(
            *(jax.tree.map(lambda part: part[side::2], pieces) for side in (0, 1))
        )
    return jax.tree.map(lambda part: part[0], pieces)


def entering_2(shard, axis, combine, identity):
    size, index = (lax.axis_size(axis), lax.axis_index(axis))
    passed = jnp.arange(size) < index

    def kept(part, zero, own):
        part = jnp.where(
            passed.reshape(-1, *(1 for _ in own.shape)),
            part.astype(own.dtype),
            jnp.asarray(zero, own.dtype),
        )
        return part

    pieces = all_in_one(
        jax.tree.map(
            lambda part, kind: part.astype(kind),
            shard,
            jax.tree.map(lambda a: jnp.bfloat16 if a.dtype == jnp.float32 else a.dtype, shard),
        ),
        axis,
    )
    return folded_in_pairs(jax.tree.map(kept, pieces, identity, shard), combine)


def matmul(left, right):
    return jnp.einsum("...ij,...jk->...ik", left, right, precision=highest)


def chain(earlier, later):
    return (matmul(earlier[0], later[0]), matmul(earlier[1], later[0]) + later[1])


def per_head_input(
    receptance,
    key_matrix,
    value_matrix,
    decay_input_term,
    decay_channel_offset,
    head_log_decay,
    context_step_logits,
):
    head_split_shape = (receptance.shape[0], head_log_decay.shape[1], HEAD_CHANNELS)
    read_vec = receptance.astype(jnp.float32).reshape(head_split_shape)
    key_vec = key_matrix.astype(jnp.float32).reshape(head_split_shape)
    value_vec = value_matrix.astype(jnp.float32).reshape(head_split_shape)
    decay_logits = (decay_input_term.astype(jnp.float32) + decay_channel_offset[None, :]).reshape(
        head_split_shape
    )
    decay_vector = jnp.exp(
        -decay_factor * jax.nn.sigmoid(decay_logits) + head_log_decay[:, :, None]
    )
    learn_vec = jax.nn.sigmoid(context_step_logits.astype(jnp.float32)).reshape(head_split_shape)
    unit_vec = key_vec * lax.rsqrt(jnp.sum(key_vec * key_vec, axis=-1, keepdims=True) + key_eps)
    return (read_vec, decay_vector, -unit_vec, unit_vec * learn_vec, key_vec * learn_vec, value_vec)


def block_prefix(transit, written, identity_mat):
    run_count = transit.shape[0] // run_len
    tail_shape = transit.shape[1:]
    runs_map = transit.reshape((run_count, run_len) + tail_shape)
    runs_state = written.reshape((run_count, run_len) + tail_shape)
    maps_list = [runs_map[:, 0]]
    states_list = [runs_state[:, 0]]
    for position in range(1, run_len):
        joined = chain(
            (maps_list[-1], states_list[-1]), (runs_map[:, position], runs_state[:, position])
        )
        maps_list.append(joined[0])
        states_list.append(joined[1])
    inner_map = jnp.stack(maps_list, axis=1)
    inner_state = jnp.stack(states_list, axis=1)
    total_map, total_state = (maps_list[-1], states_list[-1])
    enter_maps = [jnp.broadcast_to(identity_mat, tail_shape)]
    enter_states = [jnp.zeros(tail_shape, jnp.float32)]
    for position in range(1, run_count):
        joined = chain(
            (enter_maps[-1], enter_states[-1]), (total_map[position - 1], total_state[position - 1])
        )
        enter_maps.append(joined[0])
        enter_states.append(joined[1])
    enter_map = jnp.stack(enter_maps, axis=0)[:, None]
    enter_state = jnp.stack(enter_states, axis=0)[:, None]
    prefix_map = matmul(enter_map, inner_map)
    prefix_state = matmul(enter_state, inner_map) + inner_state
    return (prefix_map.reshape(transit.shape), prefix_state.reshape(transit.shape))


def local_pass(input_rows):
    token_count, head_count, head_width = input_rows[0].shape
    block_count = token_count // block_len
    identity_mat = jnp.eye(head_width, dtype=jnp.float32)

    def one_block(carried, packed):
        through_map, state_mat = carried
        read_vec, decay_vector, erase_vec, write_vec, keyed_vec, value_vec = packed
        transit = (
            decay_vector[..., None, :] * identity_mat
            + erase_vec[..., :, None] * write_vec[..., None, :]
        )
        written = value_vec[..., :, None] * keyed_vec[..., None, :]
        prefix_map, prefix_state = block_prefix(transit, written, identity_mat)
        seen_vec = jnp.einsum("thij,thj->thi", prefix_map, read_vec, precision=highest)
        through = jnp.einsum("hij,thj->thi", through_map, seen_vec, precision=highest)
        local_out = jnp.einsum("hij,thj->thi", state_mat, seen_vec, precision=highest)
        local_out = local_out + jnp.einsum(
            "thij,thj->thi", prefix_state, read_vec, precision=highest
        )
        through_map = matmul(through_map, prefix_map[-1])
        state_mat = matmul(state_mat, prefix_map[-1]) + prefix_state[-1]
        return ((through_map, state_mat), (local_out, through))

    start_map = jnp.broadcast_to(identity_mat, (head_count, head_width, head_width))
    start_state = jnp.zeros((head_count, head_width, head_width), jnp.float32)
    blocked = tuple(
        (item.reshape(block_count, block_len, head_count, head_width) for item in input_rows)
    )
    final, outputs = lax.scan(one_block, (start_map, start_state), blocked)
    local_out = outputs[0].reshape(token_count, head_count, head_width)
    through = outputs[1].reshape(token_count, head_count, head_width)
    return (final, local_out, through)


def finish(mixer_out, head_norm_scale, head_gate_rows):
    average = jnp.mean(mixer_out, axis=-1, keepdims=True)
    centred = mixer_out - average
    spread = jnp.mean(centred * centred, axis=-1, keepdims=True)
    normed = (centred * lax.rsqrt(spread + group_eps)).reshape(mixer_out.shape[0], -1)
    return (normed * head_norm_scale[None, :] * head_gate_rows.astype(jnp.float32)).astype(
        jnp.bfloat16
    )


def dispatch_tables(chosen, experts, capacity):
    row_count = chosen.shape[0]
    flat_ids = chosen.reshape(-1)
    matches = (flat_ids[:, None] == jnp.arange(experts, dtype=jnp.int32)[None, :]).astype(jnp.int32)
    slot_of = jnp.sum(jnp.cumsum(matches, axis=0) * matches, axis=1) - 1
    placing = flat_ids * capacity + slot_of
    routing = jnp.arange(experts * capacity, dtype=jnp.int32)[:, None] == placing[None, :]
    spread_rows = jnp.any(routing.reshape(experts * capacity, row_count, chosen.shape[1]), axis=2)
    return (spread_rows.astype(jnp.bfloat16), routing.astype(jnp.bfloat16))


def expand(rows_in, gate_mat, up_mat):
    gate_act = jnp.dot(rows_in, gate_mat, preferred_element_type=jnp.float32)
    up_act = jnp.dot(rows_in, up_mat, preferred_element_type=jnp.float32)
    return (jax.nn.silu(gate_act) * up_act).astype(jnp.bfloat16)


def shards(
    receptance,
    key_matrix,
    value_matrix,
    decay_input_term,
    decay_channel_offset,
    head_log_decay,
    context_step_logits,
    head_gate_rows,
    head_norm_scale,
    mixer_output_weight,
    residual,
    expert_norm_scale,
    expert_index_table,
    expert_router_scores,
    expert_gate_weight,
    expert_up_weight,
    expert_down_weight,
):
    input_rows = per_head_input(
        receptance,
        key_matrix,
        value_matrix,
        decay_input_term,
        decay_channel_offset,
        head_log_decay,
        context_step_logits,
    )
    final, local_out, through = local_pass(input_rows)
    start_map = jnp.broadcast_to(jnp.eye(final[0].shape[1], dtype=jnp.float32), final[0].shape)
    entering = entering_2(final, "sp", chain, (start_map, jnp.zeros_like(final[1])))
    mixer_out = local_out + jnp.einsum("hij,thj->thi", entering[1], through, precision=highest)
    attended = finish(mixer_out, head_norm_scale, head_gate_rows)
    row_count = residual.shape[0]
    token_rows = lax.all_to_all(attended, "tp", split_axis=0, concat_axis=1, tiled=True)
    projected = jnp.dot(token_rows, mixer_output_weight, preferred_element_type=jnp.float32)
    mixed = (residual.astype(jnp.float32) + projected).astype(jnp.bfloat16)
    mixed_f = mixed.astype(jnp.float32)
    normed = (
        mixed_f
        * lax.rsqrt(jnp.mean(mixed_f * mixed_f, axis=-1, keepdims=True) + norm_eps)
        * expert_norm_scale[None, :]
    ).astype(jnp.bfloat16)
    model_width = normed.shape[1]
    sp_size = lax.axis_size("sp")
    experts = sp_size * expert_gate_weight.shape[0]
    capacity = 2 * row_count * TOPK // experts
    gate_mat, up_mat, down_mat = (expert_gate_weight[0], expert_up_weight[0], expert_down_weight[0])
    spread_own, routing = dispatch_tables(expert_index_table, experts, capacity)
    outgoing = jnp.dot(spread_own, normed, preferred_element_type=jnp.float32).astype(jnp.bfloat16)
    outgoing = outgoing.reshape(experts, capacity, model_width)
    incoming = lax.all_to_all(outgoing, "sp", split_axis=0, concat_axis=0, tiled=True).reshape(
        sp_size * capacity, model_width
    )
    hidden = expand(lax.all_gather(incoming, "tp", axis=0, tiled=True), gate_mat, up_mat)
    summed = lax.psum_scatter(
        jnp.dot(hidden, down_mat, preferred_element_type=jnp.float32).astype(jnp.bfloat16),
        "tp",
        scatter_dimension=0,
        tiled=True,
    )
    returned = lax.all_to_all(
        summed.reshape(sp_size, capacity, model_width),
        "sp",
        split_axis=0,
        concat_axis=0,
        tiled=True,
    )
    pair_out = jnp.einsum(
        "sp,sd->pd",
        routing,
        returned.reshape(experts * capacity, model_width),
        preferred_element_type=jnp.float32,
    ).reshape(row_count, TOPK, model_width)
    weights = jax.nn.sigmoid(expert_router_scores - expert_router_scores[:, ::-1])
    total = mixed_f + jnp.sum(weights[:, :, None] * pair_out, axis=1)
    return total.astype(jnp.bfloat16)


def solution(mesh):
    return jax.shard_map(
        shards,
        mesh=mesh,
        in_specs=(
            P("sp", "tp"),
            P("sp", "tp"),
            P("sp", "tp"),
            P("sp", "tp"),
            P("tp"),
            P("sp", "tp"),
            P("sp", "tp"),
            P("sp", "tp"),
            P("tp"),
            P(),
            P(("sp", "tp"), None),
            P(),
            P(("sp", "tp"), None),
            P(("sp", "tp"), None),
            P("sp", None, "tp"),
            P("sp", None, "tp"),
            P("sp", "tp", None),
        ),
        out_specs=P(("sp", "tp"), None),
        check_vma=False,
    )
```

profile of v0, /device:TPU:1, one launch (start us, length us, event | category | flops | bytes accessed | tf_op | source)
XLA Modules:
  0.0 324.5 jit_solution(15892293677438229831)
XLA Ops:
  11.3 126.3 %while.18 = (s32[]{:T(128)}, f32[1,64,64]{1,2,0:T(8,128)S(1)}, f32[1,64,64]{1,2,0:T(8,128)S(1)}, f32[4,64,1,64]{3,1,2,0:T(8,128)}, f32[4,64,1,64]{3,1,2,0:T(8,12...) while((s32[]{:T(128)}, f32[1,64,64]{1,2,0:T(8,128)S(1)}, ...), condition=%wide.region_2.3_spmd.clone.clone, body=%wide.region_1.2_spmd.clone.clone.sunk | while | flops 819490816 | bytes 49071324 | solution.py:164
  19.7 2.0 bitcast_add_fusion.2
  21.8 1.1 copy-done.1
  23.0 3.4 %fusion.242 = f32[64,1,64]{2,1,0:T(1,128)S(1)} fusion(f32[64,64,64]{2,1,0:T(8,128)S(1)} %bitcast.685, f32[4,64,1,64]{3,2,1,0:T(1,128)S(1)} %get-tuple-element.409, s32[]{:T(128)} %get-tuple-element.387), kind=kOutput, calls=%fused_computation.106.clone.1 | convolution fusion | flops 3145728 | bytes 2146308 | tf_op jit(solution)/shard_map/while/body/eval_jaxpr/thij,thj->thi/dot_general | solution.py:152
  28.2 5.0 %fusion.239 = f32[8,8,64,64]{3,2,1,0:T(8,128)S(1)} fusion(f32[8,1,64,64]{2,3,1,0:T(8,128)S(1)} %fusion.238, f32[8,8,1,64,64]{4,3,0,2,1:T(8,128)} %copy-done.2), kind=kOutput, calls=%fused_computation.2.clone.1 | convolution fusion | flops 201326592 | bytes 2228224 | tf_op jit(solution)/shard_map/while/body/eval_jaxpr/...ij,...jk->...ik/dot_general | solution.py:73
  33.3 1.3 copy-done.3
  34.6 1.9 fusion.243
  37.3 2.9 copy.216
  40.2 0.9 fusion.241
  51.2 2.0 bitcast_add_fusion.2
  53.4 1.1 copy-done.1
  54.5 3.4 %fusion.242 = f32[64,1,64]{2,1,0:T(1,128)S(1)} fusion(f32[64,64,64]{2,1,0:T(8,128)S(1)} %bitcast.685, f32[4,64,1,64]{3,2,1,0:T(1,128)S(1)} %get-tuple-element.409, s32[]{:T(128)} %get-tuple-element.387), kind=kOutput, calls=%fused_computation.106.clone.1 | convolution fusion | flops 3145728 | bytes 2146308 | tf_op jit(solution)/shard_map/while/body/eval_jaxpr/thij,thj->thi/dot_general | solution.py:152
  59.8 5.0 %fusion.239 = f32[8,8,64,64]{3,2,1,0:T(8,128)S(1)} fusion(f32[8,1,64,64]{2,3,1,0:T(8,128)S(1)} %fusion.238, f32[8,8,1,64,64]{4,3,0,2,1:T(8,128)} %copy-done.2), kind=kOutput, calls=%fused_computation.2.clone.1 | convolution fusion | flops 201326592 | bytes 2228224 | tf_op jit(solution)/shard_map/while/body/eval_jaxpr/...ij,...jk->...ik/dot_general | solution.py:73
  64.8 1.3 copy-done.3
  66.1 1.9 fusion.243
  68.8 2.9 copy.216
  71.7 0.9 fusion.241
  82.7 2.0 bitcast_add_fusion.2
  84.9 1.1 copy-done.1
  86.1 3.4 %fusion.242 = f32[64,1,64]{2,1,0:T(1,128)S(1)} fusion(f32[64,64,64]{2,1,0:T(8,128)S(1)} %bitcast.685, f32[4,64,1,64]{3,2,1,0:T(1,128)S(1)} %get-tuple-element.409, s32[]{:T(128)} %get-tuple-element.387), kind=kOutput, calls=%fused_computation.106.clone.1 | convolution fusion | flops 3145728 | bytes 2146308 | tf_op jit(solution)/shard_map/while/body/eval_jaxpr/thij,thj->thi/dot_general | solution.py:152
  91.3 5.0 %fusion.239 = f32[8,8,64,64]{3,2,1,0:T(8,128)S(1)} fusion(f32[8,1,64,64]{2,3,1,0:T(8,128)S(1)} %fusion.238, f32[8,8,1,64,64]{4,3,0,2,1:T(8,128)} %copy-done.2), kind=kOutput, calls=%fused_computation.2.clone.1 | convolution fusion | flops 201326592 | bytes 2228224 | tf_op jit(solution)/shard_map/while/body/eval_jaxpr/...ij,...jk->...ik/dot_general | solution.py:73
  96.3 1.3 copy-done.3
  97.7 1.9 fusion.243
  100.4 2.9 copy.216
  103.3 0.9 fusion.241
  105.0 0.9 convolution_bitcast_fusion.12
  114.3 2.0 bitcast_add_fusion.2
  116.4 1.1 copy-done.1
  117.6 3.4 %fusion.242 = f32[64,1,64]{2,1,0:T(1,128)S(1)} fusion(f32[64,64,64]{2,1,0:T(8,128)S(1)} %bitcast.685, f32[4,64,1,64]{3,2,1,0:T(1,128)S(1)} %get-tuple-element.409, s32[]{:T(128)} %get-tuple-element.387), kind=kOutput, calls=%fused_computation.106.clone.1 | convolution fusion | flops 3145728 | bytes 2146308 | tf_op jit(solution)/shard_map/while/body/eval_jaxpr/thij,thj->thi/dot_general | solution.py:152
  122.8 5.0 %fusion.239 = f32[8,8,64,64]{3,2,1,0:T(8,128)S(1)} fusion(f32[8,1,64,64]{2,3,1,0:T(8,128)S(1)} %fusion.238, f32[8,8,1,64,64]{4,3,0,2,1:T(8,128)} %copy-done.2), kind=kOutput, calls=%fused_computation.2.clone.1 | convolution fusion | flops 201326592 | bytes 2228224 | tf_op jit(solution)/shard_map/while/body/eval_jaxpr/...ij,...jk->...ik/dot_general | solution.py:73
  127.9 1.3 copy-done.3
  129.2 1.9 fusion.243
  131.9 2.9 copy.216
  134.8 0.9 fusion.241
  138.5 7.6 %all-to-all-start = ((bf16[16,128,64]{1,2,0:T(8,128)(2,1)}), bf16[16,128,64]{1,2,0:T(8,128)(2,1)S(1)}, u32[]{:S(2)}, u32[]{:S(2)}) async-start(bf16[16,128,64]{1,2,0:T(8,128)(2,1)} %broadcast_in_dim.38), calls=%async_computation | async-start | bytes 524288 | tf_op jit(solution)/shard_map/all_to_all | solution.py:21
  146.6 1.0 copy.180
  147.8 5.8 %all-to-all-done = bf16[16,128,64]{1,2,0:T(8,128)(2,1)S(1)} async-done(((bf16[16,128,64]{1,2,0:T(8,128)(2,1)}), bf16[16,128,64]{1,2,0:T(8,128)(2,1)S(1)}, u32[]{:S(2)}, u32[]{:S(2)}) %all-to-all-start) | async-done | bytes 262176 | tf_op jit(solution)/shard_map/all_to_all | solution.py:21
  157.5 10.6 %all-to-all-start.1 = ((bf16[16,2,512]{2,1,0:T(2,128)(2,1)}), bf16[16,2,512]{2,1,0:T(2,128)(2,1)S(1)}, u32[]{:S(2)}, u32[]{:S(2)}) async-start(bf16[16,2,512]{2,1,0:T(2,128)(2,1)} %reshape.690), calls=%async_computation.1 | async-start | bytes 65536 | tf_op jit(solution)/shard_map/all_to_all | solution.py:231
  168.2 7.3 %all-to-all-done.1 = bf16[16,2,512]{2,1,0:T(2,128)(2,1)S(1)} async-done(((bf16[16,2,512]{2,1,0:T(2,128)(2,1)}), bf16[16,2,512]{2,1,0:T(2,128)(2,1)S(1)}, u32[]{:S(2)}, u32[]{:S(2)}) %all-to-all-start.1) | async-done | bytes 32800 | tf_op jit(solution)/shard_map/all_to_all | solution.py:231
  175.7 3.0 multiply_reduce_fusion
  179.1 10.7 %all_to_all.34 = bf16[16,4,2048]{2,1,0:T(4,128)(2,1)S(1)} all-to-all(bf16[16,4,2048]{2,1,0:T(4,128)(2,1)S(1)} %reshape.623), channel_id=1, replica_groups=mesh['sp'=16,'tp'=16] {'sp'}, dimensions={0} | all-to-all | bytes 524288 | tf_op jit(solution)/shard_map/all_to_all | solution.py:248
  190.7 35.9 %all-gather.2.cloned.1.call-done = bf16[1024,2048]{1,0:T(8,128)(2,1)} async-done(((bf16[64,2048]{1,0:T(8,128)(2,1)}), bf16[1024,2048]{1,0:T(8,128)(2,1)}) %all-gather.2.cloned.1.call-update) | async-done | bytes 4194320 | tf_op jit(solution)/shard_map/all_gather | solution.py:251
  226.5 6.1 %fusion.53 = f32[1024,448]{0,1:T(8,128)} fusion(bf16[1024,2048]{1,0:T(8,128)(2,1)} %all-gather.2.cloned.1.call-done, bf16[1,2048,448]{1,2,0:T(8,128)(2,1)} %param.33), kind=kOutput, calls=%fused_computation.143 | convolution fusion | flops 1879048192 | bytes 7864320 | tf_op jit(solution)/shard_map/dot_general | solution.py:192
  232.7 9.7 %convolution_convert_fusion = bf16[1024,2048]{1,0:T(8,128)(2,1)} fusion(bf16[1,448,2048]{2,1,0:T(8,128)(2,1)S(1)} %copy-done, f32[1024,448]{0,1:T(8,128)} %fusion.53, bf16[1024,2048]{1,0:T(8,128)(2,1)} %all-gather.2.cloned.1.call-done, bf16[1,2048,448]{1,2,0:T(8,128)(2,1)} %param.34), kind=kOutput, calls=%fused_computation.134 | convolution fusion | flops 3762946048 | bytes 13893632 | tf_op jit(solution)/shard_map/dot_general | solution.py:253
  242.4 58.5 %reduce-scatter.2.cloned.1.call-done = bf16[64,2048]{1,0:T(8,128)(2,1)} async-done(((bf16[1024,2048]{1,0:T(8,128)(2,1)}), bf16[64,2048]{1,0:T(8,128)(2,1)}) %reduce-scatter.2.cloned.1.call-update) | async-done | bytes 262160 | tf_op jit(solution)/shard_map/reduce_scatter | solution.py:252
  300.9 1.8 reshape.625
  302.7 6.6 %all-to-all-start.3 = ((bf16[16,4,2048]{2,1,0:T(4,128)(2,1)}), bf16[16,4,2048]{2,1,0:T(4,128)(2,1)S(1)}, u32[]{:S(2)}, u32[]{:S(2)}) async-start(bf16[16,4,2048]{2,1,0:T(4,128)(2,1)} %reshape.625), calls=%async_computation.4 | async-start | bytes 524288 | tf_op jit(solution)/shard_map/all_to_all | solution.py:258
  309.4 7.4 %all-to-all-done.3 = bf16[16,4,2048]{2,1,0:T(4,128)(2,1)S(1)} async-done(((bf16[16,4,2048]{2,1,0:T(4,128)(2,1)}), bf16[16,4,2048]{2,1,0:T(4,128)(2,1)S(1)}, u32[]{:S(2)}, u32[]{:S(2)}) %all-to-all-start.3) | async-done | bytes 262176 | tf_op jit(solution)/shard_map/all_to_all | solution.py:258
  (336 shorter events, 61.5 us)
Async XLA Ops:
  6.5 226.1 %copy-start = (bf16[1,448,2048]{2,1,0:T(8,128)(2,1)S(1)}, bf16[1,448,2048]{2,1,0:T(8,128)(2,1)}, u32[]{:S(2)}) copy-start(bf16[1,448,2048]{2,1,0:T(8,128)(2,1)} %param.35) | copy-start | bytes 5505028
  11.3 134.8 %copy-start.8 = (s32[16,2]{0,1:T(2,128)S(1)}, s32[16,2]{0,1:T(2,128)}, u32[]{:S(2)}) copy-start(s32[16,2]{0,1:T(2,128)} %param.31) | copy-start | bytes 388
  18.5 3.2 copy-start.2
  21.7 1.3 copy-start.1
  33.3 1.3 copy-start.3
  50.0 3.2 copy-start.2
  53.2 1.3 copy-start.1
  64.8 1.3 copy-start.3
  81.5 3.2 copy-start.2
  84.8 1.3 copy-start.1
  96.3 1.3 copy-start.3
  113.1 3.2 copy-start.2
  116.3 1.3 copy-start.1
  127.9 1.3 copy-start.3
  138.5 15.1 %all-to-all-start = ((bf16[16,128,64]{1,2,0:T(8,128)(2,1)}), bf16[16,128,64]{1,2,0:T(8,128)(2,1)S(1)}, u32[]{:S(2)}, u32[]{:S(2)}) async-start(bf16[16,128,64]{1,2,0:T(8,128)(2,1)} %broadcast_in_dim.38), calls=%async_computation | async-start | bytes 524288 | tf_op jit(solution)/shard_map/all_to_all | solution.py:21
  154.1 2.0 copy-start.4
  154.1 2.4 copy-start.6
  154.2 2.4 copy-start.10
  154.3 21.4 %copy-start.5 = (bf16[16,2048]{1,0:T(8,128)(2,1)S(1)}, bf16[16,2048]{1,0:T(8,128)(2,1)}, u32[]{:S(2)}) copy-start(bf16[16,2048]{1,0:T(8,128)(2,1)} %param.29) | copy-start | bytes 196612
  157.5 18.0 %all-to-all-start.1 = ((bf16[16,2,512]{2,1,0:T(2,128)(2,1)}), bf16[16,2,512]{2,1,0:T(2,128)(2,1)S(1)}, u32[]{:S(2)}, u32[]{:S(2)}) async-start(bf16[16,2,512]{2,1,0:T(2,128)(2,1)} %reshape.690), calls=%async_computation.1 | async-start | bytes 65536 | tf_op jit(solution)/shard_map/all_to_all | solution.py:231
  168.1 58.5 %all-gather.2.cloned.1.call-start = ((), (), s32[]{:S(2)}) async-start(), calls=%async_computation.5 | async-start | bytes 4456448 | tf_op jit(solution)/shard_map/all_gather | solution.py:251
  175.7 3.0 copy-start.7
  190.6 110.3 %reduce-scatter.2.cloned.1.call-start = ((), (), s32[]{:S(2)}) async-start(), calls=%async_computation.6 | async-start | bytes 4456448 | tf_op jit(solution)/shard_map/reduce_scatter | solution.py:252
  242.4 67.0 %copy-start.9 = (f32[16,2]{0,1:T(2,128)S(1)}, f32[16,2]{0,1:T(2,128)}, u32[]{:S(2)}) copy-start(f32[16,2]{0,1:T(2,128)} %param.32) | copy-start | bytes 388
  302.7 14.1 %all-to-all-start.3 = ((bf16[16,4,2048]{2,1,0:T(4,128)(2,1)}), bf16[16,4,2048]{2,1,0:T(4,128)(2,1)S(1)}, u32[]{:S(2)}, u32[]{:S(2)}) async-start(bf16[16,4,2048]{2,1,0:T(4,128)(2,1)} %reshape.625), calls=%async_computation.4 | async-start | bytes 524288 | tf_op jit(solution)/shard_map/all_to_all | solution.py:258
Sparse Core Ops, SparseCore 0:
  190.7 35.7 all-gather.1
  242.5 58.3 reduce-scatter.1
where the time goes:
time: 329 us; the launch traced here: 325 us
  matrix products  116 us (35%)
  waiting for transfers between devices  115 us (35%)
  local copies, waits for them, and re-layouts  33.2 us (10%)
  starting transfers between devices  24.8 us (8%)
  between operations  13.8 us (4%)
  blocking collectives  10.7 us (3%)
  other arithmetic  9.22 us (3%)
    dot_general x134, matrix products, matmul(): return jnp.einsum('...ij,...jk->...ik', left, right, precision=highest)  68.9 us
    reduce_scatter x1, waiting for transfers between devices, shards(): lax.psum_scatter(jnp.dot(hidden, down_mat, preferred_element_type=jnp.flo...  58.5 us
    all_gather x1, waiting for transfers between devices, shards(): lax.all_gather(incoming, 'tp', axis=0, tiled=True)  35.9 us
    dot_general x4, matrix products, one_block(): jnp.einsum('thij,thj->thi', prefix_state, read_vec, precision=highest)  13.4 us
    add x8, local copies, waits for them, and re-layouts, block_prefix(): prefix_state = matmul(enter_state, inner_map) + inner_state  12.2 us
    all_to_all x1, blocking collectives, shards(): lax.all_to_all(outgoing, 'sp', split_axis=0, concat_axis=0, tiled=True)  10.7 us
    all_to_all x1, starting transfers between devices, shards(): lax.all_to_all(attended, 'tp', split_axis=0, concat_axis=1, tiled=True)  10.6 us
    while x64, local copies, waits for them, and re-layouts  10.2 us
  transfers between devices with their start and end apart: 5, of which 5 were waited for; matrix products, arithmetic and copies ran while one was open for 1% of the time, Pallas kernels for 0%

commit v1 on v0

v1 whole, which is shorter than its diff:
```python
import jax
import jax.numpy as jnp
from jax import lax
from jax.experimental import pallas as pl
from jax.experimental.pallas import tpu as pltpu
from jax.sharding import PartitionSpec as P

HEAD_CHANNELS = 64
TOPK = 2


decay_factor = 0.6065306597126334
group_eps = 0.00064
norm_eps = 1e-06
key_eps = 1e-06
highest = lax.Precision.HIGHEST
block_len = 64
run_len = 8


def copy_for_each(shard, axis):
    copies = jnp.broadcast_to(shard, (lax.axis_size(axis), *shard.shape))
    return lax.all_to_all(copies, axis, split_axis=0, concat_axis=0, tiled=True)


def all_in_one(shard, axis):
    leaves = jax.tree.leaves(shard)
    order = sorted(range(len(leaves)), key=lambda k: -leaves[k].size)
    width = (1, *leaves[order[0]].shape)[-1]
    lines = [
        jnp.pad(leaves[k].reshape(-1), (0, -leaves[k].size % width)).reshape(-1, width)
        for k in order
    ]
    both, at, found = (copy_for_each(jnp.concatenate(lines), axis), 0, {})
    for k, line in zip(order, lines):
        share = both[:, at : at + len(line)].reshape(len(both), -1)
        found[k] = share[:, : leaves[k].size].reshape(-1, *leaves[k].shape)
        at += len(line)
    numbers = iter(range(len(leaves)))
    return jax.tree.map(lambda _: found[next(numbers)], shard)


def folded_in_pairs(pieces, combine):
    while len(jax.tree.leaves(pieces)[0]) > 1:
        pieces = jax.vmap(combine)(
            *(jax.tree.map(lambda part: part[side::2], pieces) for side in (0, 1))
        )
    return jax.tree.map(lambda part: part[0], pieces)


def entering_2(shard, axis, combine, identity):
    size, index = (lax.axis_size(axis), lax.axis_index(axis))
    passed = jnp.arange(size) < index

    def kept(part, zero, own):
        part = jnp.where(
            passed.reshape(-1, *(1 for _ in own.shape)),
            part.astype(own.dtype),
            jnp.asarray(zero, own.dtype),
        )
        return part

    pieces = all_in_one(
        jax.tree.map(
            lambda part, kind: part.astype(kind),
            shard,
            jax.tree.map(lambda a: jnp.bfloat16 if a.dtype == jnp.float32 else a.dtype, shard),
        ),
        axis,
    )
    return folded_in_pairs(jax.tree.map(kept, pieces, identity, shard), combine)


def matmul(left, right):
    return jnp.einsum("...ij,...jk->...ik", left, right, precision=highest)


def chain(earlier, later):
    return (matmul(earlier[0], later[0]), matmul(earlier[1], later[0]) + later[1])


seq_len = 256
chunk_len = 32
chunks = seq_len // chunk_len


def split_two(value):
    top = value.astype(jnp.bfloat16)
    return top, (value - top.astype(jnp.float32)).astype(jnp.bfloat16)


def dot_f32(left, right, dims=(((1,), (0,)), ((), ()))):
    return lax.dot_general(left, right, dims, preferred_element_type=jnp.float32)


def product(left, right):
    left_top, left_low = split_two(left)
    right_top, right_low = split_two(right)
    return dot_f32(
        jnp.concatenate([left_top, left_top, left_low], axis=1),
        jnp.concatenate([right_top, right_low, right_top], axis=0),
    )


def product_nt(left, right):
    left_top, left_low = split_two(left)
    right_top, right_low = split_two(right)
    return dot_f32(
        jnp.concatenate([left_top, left_top, left_low], axis=1),
        jnp.concatenate([right_top, right_low, right_top], axis=1),
        (((1,), (1,)), ((), ())),
    )


def sigmoid(value):
    return 1.0 / (1.0 + jnp.exp(-value))


def mixer_local(receptance, key_matrix, value_matrix, decay_input, decay_offset, head_decay, step_logits):
    key_vec = key_matrix.astype(jnp.float32)
    read_vec = receptance.astype(jnp.float32)
    log_decay = head_decay - decay_factor * sigmoid(decay_input.astype(jnp.float32) + decay_offset)
    learn = sigmoid(step_logits.astype(jnp.float32))
    unit = key_vec * lax.rsqrt(jnp.sum(key_vec * key_vec, axis=1, keepdims=True) + key_eps)
    write = unit * learn
    keyed = key_vec * learn

    row = lax.broadcasted_iota(jnp.int32, (seq_len, seq_len), 0)
    col = lax.broadcasted_iota(jnp.int32, (seq_len, seq_len), 1)
    same = (row >> 5) == (col >> 5)
    upto = same & (col <= row)
    before = same & (col < row)

    log_top, log_rest = split_two(log_decay)
    log_low = (log_decay - log_top.astype(jnp.float32) - log_rest.astype(jnp.float32)).astype(jnp.bfloat16)
    summed = dot_f32(
        jnp.where(upto, 1.0, 0.0).astype(jnp.bfloat16),
        jnp.concatenate([log_top, log_rest, log_low], axis=1),
    )
    total = summed[:, :64] + summed[:, 64:128] + summed[:, 128:192]
    by_chunk = total.reshape(chunks, chunk_len, HEAD_CHANNELS)
    middle = jnp.broadcast_to(by_chunk[:, chunk_len // 2 - 1 : chunk_len // 2], by_chunk.shape).reshape(total.shape)
    last = by_chunk[:, chunk_len - 1 : chunk_len]
    ending = jnp.broadcast_to(last, by_chunk.shape).reshape(total.shape)
    prior = total - log_decay

    up_scale = jnp.exp(middle - total)
    gram = product_nt(
        jnp.concatenate([-unit * jnp.exp(prior - middle), read_vec * jnp.exp(total - middle)], axis=0),
        jnp.concatenate([write * up_scale, keyed * up_scale], axis=0),
    )
    erase_write = jnp.where(before, gram[:seq_len, :seq_len], 0.0)
    erase_keyed = jnp.where(before, gram[:seq_len, seq_len:], 0.0)
    read_write = jnp.where(upto, gram[seq_len:, :seq_len], 0.0)
    read_keyed = jnp.where(upto, gram[seq_len:, seq_len:], 0.0)

    def below(width):
        return (
            ((row & (-2 * width)) == (col & (-2 * width)))
            & ((row & width) != 0)
            & ((col & width) == 0)
        )

    solved = jnp.where(row == col, 1.0, 0.0) + jnp.where(below(1), erase_write, 0.0)
    for width in (2, 4, 8, 16):
        solved = solved + product(solved, product(jnp.where(below(width), erase_write, 0.0), solved))

    stacked_top, stacked_low = split_two(jnp.concatenate([erase_keyed, read_keyed], axis=0))
    on_values = dot_f32(
        jnp.concatenate([stacked_top, stacked_low], axis=1),
        jnp.concatenate([value_matrix, value_matrix], axis=0),
    )
    erased = product(
        solved, jnp.concatenate([-unit * jnp.exp(prior), on_values[:seq_len]], axis=1)
    )
    shown = product(read_write, erased)
    seen = read_vec * jnp.exp(total) + shown[:, :64]
    own = shown[:, 64:] + on_values[seq_len:]

    tail_scale = jnp.exp(ending - total)
    wide_row = lax.broadcasted_iota(jnp.int32, (seq_len, chunks * 64), 0)
    wide_col = lax.broadcasted_iota(jnp.int32, (seq_len, chunks * 64), 1)
    in_block = (wide_row >> 5) == (wide_col >> 6)
    write_tail = jnp.where(in_block, jnp.concatenate([write * tail_scale] * chunks, axis=1), 0.0)
    keyed_tail = jnp.where(in_block, jnp.concatenate([keyed * tail_scale] * chunks, axis=1), 0.0)
    erased_t = jnp.transpose(erased)
    value_t = jnp.transpose(value_matrix.astype(jnp.float32)).astype(jnp.bfloat16)
    maps = product(erased_t, write_tail)
    keyed_top, keyed_low = split_two(keyed_tail)
    adds = maps[64:] + dot_f32(
        jnp.concatenate([value_t, value_t], axis=1),
        jnp.concatenate([keyed_top, keyed_low], axis=0),
    )
    small_row = lax.broadcasted_iota(jnp.int32, (64, 64), 0)
    small_col = lax.broadcasted_iota(jnp.int32, (64, 64), 1)
    eye = small_row == small_col

    through = [seen[:chunk_len]]
    local = [own[:chunk_len]]
    carried = None
    for c in range(chunks):
        step_map = maps[:64, c * 64 : (c + 1) * 64] + jnp.where(eye, jnp.exp(last[c]), 0.0)
        step_add = adds[:, c * 64 : (c + 1) * 64]
        if c == 0:
            carried = jnp.concatenate([step_map, step_add], axis=0)
        else:
            part = slice(c * chunk_len, (c + 1) * chunk_len)
            viewed = product_nt(seen[part], carried)
            through.append(viewed[:, :64])
            local.append(viewed[:, 64:] + own[part])
            moved = product(carried, step_map)
            carried = jnp.concatenate([moved[:64], moved[64:] + step_add], axis=0)
    return jnp.concatenate(through, axis=0), jnp.concatenate(local, axis=0), carried


def mixer_kernel(r_ref, k_ref, v_ref, d_ref, o_ref, h_ref, c_ref, through_ref, local_ref, final_ref):
    through, local, final = mixer_local(
        r_ref[...], k_ref[...], v_ref[...], d_ref[...], o_ref[...], h_ref[...], c_ref[...]
    )
    through_ref[...] = through
    local_ref[...] = local
    final_ref[...] = final


def run_mixer(*args):
    rows = jax.ShapeDtypeStruct((seq_len, HEAD_CHANNELS), jnp.float32)
    return pl.pallas_call(
        mixer_kernel,
        out_shape=(rows, rows, jax.ShapeDtypeStruct((128, 64), jnp.float32)),
    )(*args)


def finish(mixer_out, head_norm_scale, head_gate_rows):
    average = jnp.mean(mixer_out, axis=-1, keepdims=True)
    centred = mixer_out - average
    spread = jnp.mean(centred * centred, axis=-1, keepdims=True)
    normed = (centred * lax.rsqrt(spread + group_eps)).reshape(mixer_out.shape[0], -1)
    return (normed * head_norm_scale[None, :] * head_gate_rows.astype(jnp.float32)).astype(
        jnp.bfloat16
    )


MESH = pl.DeviceIdType.MESH
sub_rows = 16
subs = 4
half = 1024
width = 2048


def place(axis_0, axis_1):
    return (axis_0, axis_1)


def transfer(source, target, send, arrive, sp, tp):
    return pltpu.make_async_remote_copy(
        src_ref=source,
        dst_ref=target,
        send_sem=send,
        recv_sem=arrive,
        device_id=(sp, tp),
        device_id_type=MESH,
    )


def ranks_of(first, second):
    count = first.shape[0]
    lane = lax.broadcasted_iota(jnp.int32, (count, 128), 1).astype(jnp.float32)
    hit_0 = jnp.where(lane == first, 1.0, 0.0)
    hit_1 = jnp.where(lane == second, 1.0, 0.0)
    row = lax.broadcasted_iota(jnp.int32, (count, count), 0)
    col = lax.broadcasted_iota(jnp.int32, (count, count), 1)
    same = (row >> 4) == (col >> 4)
    earlier = dot_f32(
        jnp.where(same & (col < row), 1.0, 0.0).astype(jnp.bfloat16),
        jnp.concatenate([hit_0, hit_1], axis=1).astype(jnp.bfloat16),
    )
    every = dot_f32(jnp.where(same, 1.0, 0.0).astype(jnp.bfloat16), hit_0.astype(jnp.bfloat16))
    rank_0 = jnp.sum(earlier[:, :128] * hit_0, axis=1, keepdims=True)
    rank_1 = jnp.sum((earlier[:, 128:] + every) * hit_1, axis=1, keepdims=True)
    return first * 16.0 + rank_0, second * 16.0 + rank_1


def one_hot_rows(source_of):
    row = lax.broadcasted_iota(jnp.int32, (256, 256), 0)
    col = lax.broadcasted_iota(jnp.int32, (256, 256), 1)
    return jnp.where(col == source_of(row), 1.0, 0.0).astype(jnp.bfloat16)


def moe_kernel(
    normed_ref,
    mixed_ref,
    table_ref,
    gate_hbm,
    up_hbm,
    down_hbm,
    out_ref,
    gate_mat,
    up_mat,
    down_mat,
    outgoing,
    incoming,
    tables,
    codes,
    rows_all,
    gate_act,
    hidden_rows,
    mine_part,
    pair_out,
    pair_in,
    leave,
    back,
    sent_sum,
    got_sum,
    weight_sem,
    table_send,
    table_recv,
    spread_send,
    spread_recv,
    ring_send,
    ring_recv,
    twin_send,
    twin_recv,
    pair_send,
    pair_recv,
    back_send,
    back_recv,
    sum_send,
    sum_recv,
):
    sp, tp = lax.axis_index("sp"), lax.axis_index("tp")
    level, core = tp // 2, tp % 2
    twin = level * 2 + (1 - core)

    loads = [
        pltpu.make_async_copy(source.at[0], target, weight_sem.at[k])
        for k, (source, target) in enumerate(
            ((gate_hbm, gate_mat), (up_hbm, up_mat), (down_hbm, down_mat))
        )
    ]
    for load in loads:
        load.start()

    barrier = pltpu.get_barrier_semaphore()
    for j in range(1, 16):
        pl.semaphore_signal(barrier, inc=1, device_id=((sp + j) % 16, tp), device_id_type=MESH)
        pl.semaphore_signal(barrier, inc=1, device_id=(sp, (tp + j) % 16), device_id_type=MESH)

    own_table = table_ref[...]
    first, second = ranks_of(own_table[:, 0:1], own_table[:, 1:2])
    lane = lax.broadcasted_iota(jnp.int32, (16, 256), 1).astype(jnp.float32)
    spread = jnp.concatenate(
        [
            jnp.where((lane == first + 4.0 * q) | (lane == second + 4.0 * q), 1.0, 0.0)
            for q in range(4)
        ],
        axis=0,
    )
    normed = normed_ref[...]
    stacked = jnp.concatenate([normed[:, q * 512 : (q + 1) * 512] for q in range(4)], axis=0)
    outgoing[...] = dot_f32(
        jnp.transpose(spread).astype(jnp.bfloat16), stacked
    ).astype(jnp.bfloat16).reshape(16, 16, 512)

    pl.semaphore_wait(barrier, 30)

    pending = []
    for j in range(1, 16):
        other = (sp + j) % 16
        copy = transfer(
            outgoing.at[other], incoming.at[sp], spread_send.at[j], spread_recv.at[sp], other, tp
        )
        copy.start()
        pending.append(copy)
    incoming[sp] = outgoing[sp]
    for j in range(1, 16):
        other = (tp + j) % 16
        copy = transfer(table_ref, tables.at[tp], table_send.at[j], table_recv.at[tp], sp, other)
        copy.start()
        pending.append(copy)
    tables[tp] = own_table

    for j in range(1, 16):
        other = (sp + j) % 16
        transfer(
            outgoing.at[other], incoming.at[other], spread_send.at[j], spread_recv.at[other], other, tp
        ).wait_recv()
    regrouped = dot_f32(
        one_hot_rows(lambda j: ((j >> 2) & 15) * 16 + (j >> 6) * 4 + (j & 3)),
        incoming[...].reshape(256, 512),
    ).astype(jnp.bfloat16)
    rows_all[tp] = jnp.concatenate([regrouped[q * 64 : (q + 1) * 64] for q in range(4)], axis=1)

    following = (((level + 1) % 8) * 2 + core, ((level + 7) % 8) * 2 + core)

    def block_at(distance, way):
        if way == 0:
            return (level + 8 - distance) % 8
        return (level + distance) % 8

    def piece_of(index, sub):
        return rows_all.at[index, pl.ds(sub * sub_rows, sub_rows)]

    def arrival(distance, sub, way):
        return (distance - 1) * subs + sub if distance < 4 else 3 * subs + sub % 2

    def travels(distance, sub, way):
        return distance < 4 or (sub < 2) == (way == 0)

    def ring(index, sub, distance, way):
        slot = arrival(distance, sub, way)
        return transfer(
            piece_of(index, sub),
            piece_of(index, sub),
            ring_send.at[way, slot],
            ring_recv.at[way, slot],
            sp,
            following[way],
        )

    def twinned(index, sub, slot):
        return transfer(
            piece_of(index, sub), piece_of(index, sub), twin_send.at[slot], twin_recv.at[slot], sp, twin
        )

    def twin_slot(distance, sub, way):
        return subs + way * 14 + arrival(distance, sub, way)

    for sub in range(subs):
        for way in (0, 1):
            copy = ring(tp, sub, 1, way)
            copy.start()
            pending.append(copy)
        copy = twinned(tp, sub, sub)
        copy.start()
        pending.append(copy)

    def forward(distance, sub):
        for way in (0, 1):
            if not travels(distance, sub, way):
                continue
            index = block_at(distance, way) * 2 + core
            ring(index, sub, distance, way).wait_recv()
            if distance < 4 and travels(distance + 1, sub, way):
                copy = ring(index, sub, distance + 1, way)
                copy.start()
                pending.append(copy)
            copy = twinned(index, sub, twin_slot(distance, sub, way))
            copy.start()
            pending.append(copy)

    def await_twin(distance):
        if distance == 4:
            for sub in range(subs):
                twinned(twin, sub, sub).wait_recv()
        for sub in range(subs):
            for way in (0, 1):
                if travels(distance, sub, way):
                    index = block_at(distance, way) * 2 + (1 - core)
                    twinned(index, sub, twin_slot(distance, sub, way)).wait_recv()

    def members(distance):
        low = block_at(distance, 0) * 2 if distance < 4 else level * 2
        high = block_at(distance, 1) * 2
        return (low, low + 1, high, high + 1)

    for j in range(1, 16):
        other = (tp + j) % 16
        transfer(
            table_ref, tables.at[other], table_send.at[j], table_recv.at[other], sp, other
        ).wait_recv()
    every = tables[...].reshape(256, 128)
    first, second = ranks_of(every[:, 0:1], every[:, 1:2])
    gap = every[:, 3:4] - every[:, 2:3]
    wide_lane = lax.broadcasted_iota(jnp.int32, (256, 128), 1)
    codes[...] = jnp.where(
        wide_lane == 0,
        first,
        jnp.where(
            wide_lane == 1,
            second,
            jnp.where(wide_lane == 2, 1.0 / (1.0 + jnp.exp(gap)), 1.0 / (1.0 + jnp.exp(-gap))),
        ),
    ).reshape(16, 16, 128)
    for load in loads:
        load.wait()

    reorder = one_hot_rows(lambda j: ((j >> 2) & 3) * 64 + (j >> 4) * 4 + (j & 3))
    core_at = pl.multiple_of(core * half, half)
    twin_at = pl.multiple_of((1 - core) * half, half)

    def rows_in(distance):
        return jnp.concatenate([rows_all[index] for index in members(distance)], axis=0)

    def stage_gate(distance):
        gate_act[...] = dot_f32(rows_in(distance), gate_mat[...])

    def stage_up(distance):
        up_act = dot_f32(rows_in(distance), up_mat[...])
        gate = gate_act[...]
        hidden = (gate / (1.0 + jnp.exp(-gate)) * up_act).astype(jnp.bfloat16)
        hidden_rows[...] = dot_f32(reorder, hidden).astype(jnp.bfloat16)

    def pair(distance):
        at = distance - 1
        return transfer(
            pair_out.at[at], pair_in.at[at], pair_send.at[at], pair_recv.at[at], sp, twin
        )

    def stage_other(distance):
        pair_out[distance - 1] = dot_f32(
            hidden_rows[...], down_mat[:, pl.ds(twin_at, half)]
        ).astype(jnp.bfloat16)
        copy = pair(distance)
        copy.start()
        pending.append(copy)

    def stage_mine(distance):
        mine_part[...] = dot_f32(hidden_rows[...], down_mat[:, pl.ds(core_at, half)])

    def stage_return(distance):
        at = distance - 1
        pair(distance).wait_recv()
        leave[at] = (
            (mine_part[...] + pair_in[at].astype(jnp.float32)).astype(jnp.bfloat16).reshape(16, 16, half)
        )
        for j in range(1, 16):
            other = (sp + j) % 16
            copy = transfer(
                leave.at[at, other],
                back.at[at, sp],
                back_send.at[at, j],
                back_recv.at[at, sp],
                other,
                tp,
            )
            copy.start()
            pending.append(copy)
        back[at, sp] = leave[at, sp]

    def stage_combine(distance):
        at = distance - 1
        for j in range(1, 16):
            other = (sp + j) % 16
            transfer(
                leave.at[at, other],
                back.at[at, other],
                back_send.at[at, j],
                back_recv.at[at, other],
                other,
                tp,
            ).wait_recv()
        parts = []
        for place_in, index in enumerate(members(distance)):
            code = codes[index]
            parts.append(
                jnp.where(lane == code[:, 0:1] + 4.0 * place_in, code[:, 2:3], 0.0)
                + jnp.where(lane == code[:, 1:2] + 4.0 * place_in, code[:, 3:4], 0.0)
            )
        top, low = split_two(jnp.concatenate(parts, axis=0))
        returned = back[at].reshape(256, half)
        sent_sum[at] = (
            (dot_f32(top, returned) + dot_f32(low, returned)).astype(jnp.bfloat16).reshape(4, 16, half)
        )
        for place_in, index in enumerate(members(distance)):
            if distance == 4 and place_in < 2:
                continue
            copy = transfer(
                sent_sum.at[at, place_in],
                got_sum.at[tp],
                sum_send.at[at, place_in],
                sum_recv.at[tp],
                sp,
                index,
            )
            copy.start()
            pending.append(copy)
        if distance == 4:
            copy = transfer(
                sent_sum.at[at, 1 - core],
                got_sum.at[tp],
                sum_send.at[at, 0],
                sum_recv.at[tp],
                sp,
                twin,
            )
            copy.start()
            pending.append(copy)
            got_sum[tp] = sent_sum[at, core]

    for sub in range(subs):
        forward(1, sub)
    for distance in (1, 2, 3):
        await_twin(distance)
        stage_gate(distance)
        forward(distance + 1, 0)
        stage_up(distance)
        forward(distance + 1, 1)
        stage_other(distance)
        forward(distance + 1, 2)
        stage_mine(distance)
        forward(distance + 1, 3)
        stage_return(distance)
        if distance > 1:
            stage_combine(distance - 1)
    await_twin(4)
    stage_gate(4)
    stage_up(4)
    stage_other(4)
    stage_mine(4)
    stage_return(4)
    stage_combine(3)
    stage_combine(4)

    for j in range(1, 16):
        other = (tp + j) % 16
        transfer(
            sent_sum.at[0, 0], got_sum.at[other], sum_send.at[0, 0], sum_recv.at[other], sp, other
        ).wait_recv()
    for side in (0, 1):
        gathered = got_sum[side].astype(jnp.float32)
        for stage in range(1, 8):
            gathered = gathered + got_sum[2 * stage + side].astype(jnp.float32)
        cut = slice(side * half, (side + 1) * half)
        out_ref[:, cut] = (mixed_ref[:, cut].astype(jnp.float32) + gathered).astype(jnp.bfloat16)
    for copy in pending:
        copy.wait_send()


def run_moe(normed, mixed, table, gate, up, down):
    vmem = pl.BlockSpec(memory_space=pltpu.VMEM)
    hbm = pl.BlockSpec(memory_space=pl.ANY)
    dma = pltpu.SemaphoreType.DMA
    return pl.pallas_call(
        moe_kernel,
        out_shape=jax.ShapeDtypeStruct((16, width), jnp.bfloat16),
        in_specs=[vmem, vmem, vmem, hbm, hbm, hbm],
        out_specs=vmem,
        scratch_shapes=[
            pltpu.VMEM((width, 448), jnp.bfloat16),
            pltpu.VMEM((width, 448), jnp.bfloat16),
            pltpu.VMEM((448, width), jnp.bfloat16),
            pltpu.VMEM((16, 16, 512), jnp.bfloat16),
            pltpu.VMEM((16, 16, 512), jnp.bfloat16),
            pltpu.VMEM((16, 16, 128), jnp.float32),
            pltpu.VMEM((16, 16, 128), jnp.float32),
            pltpu.VMEM((16, 64, width), jnp.bfloat16),
            pltpu.VMEM((256, 448), jnp.float32),
            pltpu.VMEM((256, 448), jnp.bfloat16),
            pltpu.VMEM((256, half), jnp.float32),
            pltpu.VMEM((4, 256, half), jnp.bfloat16),
            pltpu.VMEM((4, 256, half), jnp.bfloat16),
            pltpu.VMEM((4, 16, 16, half), jnp.bfloat16),
            pltpu.VMEM((4, 16, 16, half), jnp.bfloat16),
            pltpu.VMEM((4, 4, 16, half), jnp.bfloat16),
            pltpu.VMEM((16, 16, half), jnp.bfloat16),
            dma((3,)),
            dma((16,)),
            dma((16,)),
            dma((16,)),
            dma((16,)),
            dma((2, 14)),
            dma((2, 14)),
            dma((32,)),
            dma((32,)),
            dma((4,)),
            dma((4,)),
            dma((4, 16)),
            dma((4, 16)),
            dma((4, 4)),
            dma((16,)),
        ],
        compiler_params=pltpu.CompilerParams(
            collective_id=1, has_side_effects=True, vmem_limit_bytes=56 * 1024 * 1024
        ),
    )(normed, mixed, table, gate, up, down)


def shards(
    receptance,
    key_matrix,
    value_matrix,
    decay_input_term,
    decay_channel_offset,
    head_log_decay,
    context_step_logits,
    head_gate_rows,
    head_norm_scale,
    mixer_output_weight,
    residual,
    expert_norm_scale,
    expert_index_table,
    expert_router_scores,
    expert_gate_weight,
    expert_up_weight,
    expert_down_weight,
):
    through, local_out, final = run_mixer(
        receptance,
        key_matrix,
        value_matrix,
        decay_input_term,
        decay_channel_offset.reshape(1, -1),
        head_log_decay,
        context_step_logits,
    )
    through, local_out = through[:, None, :], local_out[:, None, :]
    final = (final[None, :64], final[None, 64:])
    start_map = jnp.broadcast_to(jnp.eye(final[0].shape[1], dtype=jnp.float32), final[0].shape)
    entering = entering_2(final, "sp", chain, (start_map, jnp.zeros_like(final[1])))
    mixer_out = local_out + jnp.einsum("hij,thj->thi", entering[1], through, precision=highest)
    attended = finish(mixer_out, head_norm_scale, head_gate_rows)
    row_count = residual.shape[0]
    token_rows = lax.all_to_all(attended, "tp", split_axis=0, concat_axis=1, tiled=True)
    projected = jnp.dot(token_rows, mixer_output_weight, preferred_element_type=jnp.float32)
    mixed = (residual.astype(jnp.float32) + projected).astype(jnp.bfloat16)
    mixed_f = mixed.astype(jnp.float32)
    normed = (
        mixed_f
        * lax.rsqrt(jnp.mean(mixed_f * mixed_f, axis=-1, keepdims=True) + norm_eps)
        * expert_norm_scale[None, :]
    ).astype(jnp.bfloat16)
    table = jnp.concatenate(
        [
            expert_index_table.astype(jnp.float32),
            expert_router_scores,
            jnp.zeros((row_count, 124), jnp.float32),
        ],
        axis=1,
    )
    return run_moe(normed, mixed, table, expert_gate_weight, expert_up_weight, expert_down_weight)


def solution(mesh):
    return jax.shard_map(
        shards,
        mesh=mesh,
        in_specs=(
            P("sp", "tp"),
            P("sp", "tp"),
            P("sp", "tp"),
            P("sp", "tp"),
            P("tp"),
            P("sp", "tp"),
            P("sp", "tp"),
            P("sp", "tp"),
            P("tp"),
            P(),
            P(("sp", "tp"), None),
            P(),
            P(("sp", "tp"), None),
            P(("sp", "tp"), None),
            P("sp", None, "tp"),
            P("sp", None, "tp"),
            P("sp", "tp", None),
        ),
        out_specs=P(("sp", "tp"), None),
        check_vma=False,
    )
```

time: 329 us -> 125 us (0.38)
  matrix products: 116 us -> 5.1 us
  waiting for transfers between devices: 115 us -> 5.53 us
  Pallas kernels: 0 us -> 70.7 us
  between operations: 13.8 us -> 0.25 us
  local copies, waits for them, and re-layouts: 33.2 us -> 20.7 us
  blocking collectives: 10.7 us -> 0 us
  starting transfers between devices: 24.8 us -> 18.2 us
  other arithmetic: 9.22 us -> 3.4 us
    pallas_call x0 -> x2, Pallas kernels: none -> 70.7 us  [the longest x1 63.4 us: run_moe(): pl.pallas_call(moe_kernel, out_shape=jax.ShapeDtypeStruct((16, width), jn...]
    dot_general x134 -> x6, matrix products: 68.9 us -> 1.64 us  [matmul(): return jnp.einsum('...ij,...jk->...ik', left, right, precision=highest)]
    reduce_scatter x1 -> x0, waiting for transfers between devices: 58.5 us -> none  [shards(): lax.psum_scatter(jnp.dot(hidden, down_mat, preferred_element_type=jnp.flo...]
    dot_general x20 -> x0, matrix products: 43.5 us -> none  [the longest x4 13.4 us: one_block(): jnp.einsum('thij,thj->thi', prefix_state, read_vec, precision=highest)]
    all_gather x1 -> x0, waiting for transfers between devices: 35.9 us -> none  [shards(): lax.all_gather(incoming, 'tp', axis=0, tiled=True)]
    unnamed x21 -> x29, local copies, waits for them, and re-layouts: 1.31 us -> 19.4 us
    add x8 -> x0, local copies, waits for them, and re-layouts: 12.2 us -> none  [block_prefix(): prefix_state = matmul(enter_state, inner_map) + inner_state]
    all_to_all x1 -> x0, blocking collectives: 10.7 us -> none  [shards(): lax.all_to_all(outgoing, 'sp', split_axis=0, concat_axis=0, tiled=True)]
  transfers between devices with their start and end apart: 5 -> 2, of which waited for: 5 -> 2; matrix products, arithmetic and copies ran while one was open for 1% -> 8% of each run, Pallas kernels for 0% -> 0%
where the time goes in v1:
time: 125 us; the launch traced here: 124 us
  Pallas kernels  70.7 us (57%)
  local copies, waits for them, and re-layouts  20.7 us (17%)
  starting transfers between devices  18.2 us (15%)
  waiting for transfers between devices  5.53 us (4%)
  matrix products  5.1 us (4%)
  other arithmetic  3.4 us (3%)
    pallas_call x1, Pallas kernels, run_moe(): pl.pallas_call(moe_kernel, out_shape=jax.ShapeDtypeStruct((16, width), jn...  63.4 us
    unnamed x29, local copies, waits for them, and re-layouts  19.4 us
    all_to_all x1, starting transfers between devices, shards(): lax.all_to_all(attended, 'tp', split_axis=0, concat_axis=1, tiled=True)  10.6 us
    all_to_all x1, starting transfers between devices, copy_for_each(): return lax.all_to_all(copies, axis, split_axis=0, concat_axis=0, tiled=True)  7.57 us
    pallas_call x1, Pallas kernels, run_mixer(): pl.pallas_call(mixer_kernel, out_shape=(rows, rows, jax.ShapeDtypeStruct(...  7.27 us
    all_to_all x1, waiting for transfers between devices, copy_for_each(): return lax.all_to_all(copies, axis, split_axis=0, concat_axis=0, tiled=True)  5.04 us
    dot_general x1, matrix products, shards(): jnp.dot(token_rows, mixer_output_weight, preferred_element_type=jnp.float32)  2.96 us
  transfers between devices with their start and end apart: 2, of which 2 were waited for; matrix products, arithmetic and copies ran while one was open for 8% of the time, Pallas kernels for 0%

profile of v1, /device:TPU:1, one launch (start us, length us, event | category | flops | bytes accessed | tf_op | source)
XLA Modules:
  0.0 123.8 jit_solution(8788805820198151040)
XLA Ops:
  0.0 1.5 %copy.43.r_ref = bf16[256,64]{1,0:T(8,128)(2,1)} copy(bf16[256,64]{0,1:T(8,128)(2,1)} %param.17) | data formatting | bytes 65536 | tf_op args[0]
  1.5 1.5 %copy.44.k_ref = bf16[256,64]{1,0:T(8,128)(2,1)} copy(bf16[256,64]{0,1:T(8,128)(2,1)} %param.18) | data formatting | bytes 65536 | tf_op args[1]
  3.0 1.5 %copy.45.v_ref = bf16[256,64]{1,0:T(8,128)(2,1)} copy(bf16[256,64]{0,1:T(8,128)(2,1)} %param.19) | data formatting | bytes 65536 | tf_op args[2]
  4.5 1.5 %copy.46.d_ref = bf16[256,64]{1,0:T(8,128)(2,1)} copy(bf16[256,64]{0,1:T(8,128)(2,1)} %param.20) | data formatting | bytes 65536 | tf_op args[3]
  5.9 1.5 %copy.48.c_ref = bf16[256,64]{1,0:T(8,128)(2,1)} copy(bf16[256,64]{0,1:T(8,128)(2,1)} %param.23) | data formatting | bytes 65536 | tf_op args[6]
  7.4 1.5 %copy.47.h_ref = f32[256,1]{1,0:T(8,128)} copy(f32[256,1]{0,1:T(1,128)} %param.22) | data formatting | bytes 2048 | tf_op args[5]
  8.9 7.3 %shard_map.163 = (f32[256,64]{1,0:T(8,128)}, f32[256,64]{1,0:T(8,128)}, f32[128,64]{1,0:T(8,128)}) custom-call(bf16[256,64]{1,0:T(8,128)(2,1)} %copy.43.r_ref, bf16[256,64]{1,0:T(8,128)(2,1)} %copy.44.k_ref, bf16[256,64]{1,0:T(8,128)(2,1)} %copy.45.v_ref, bf16[256,64]{1,0:T(8,128)(2,1)} %copy.46.d_ref, f32[1,64]{1,0:T(1,128)} %bitcast.76, ...), custom_call_target="tpu_custom_call" | custom-call | tf_op jit(solution)/shard_map/pallas_call | solution.py:227
  16.2 0.8 convert.4
  17.0 0.1 copy.49
  17.1 0.8 broadcast_in_dim.36
  17.9 7.6 %all-to-all-start = ((bf16[16,128,64]{1,2,0:T(8,128)(2,1)}), bf16[16,128,64]{1,2,0:T(8,128)(2,1)S(1)}, u32[]{:S(2)}, u32[]{:S(2)}) async-start(bf16[16,128,64]{1,2,0:T(8,128)(2,1)} %broadcast_in_dim.36), calls=%async_computation | async-start | bytes 524288 | tf_op jit(solution)/shard_map/all_to_all | solution.py:23
  25.4 0.7 convert_element_type.45
  26.1 0.1 copy.55
  26.2 0.8 copy.56
  27.0 0.9 copy.53
  27.8 0.1 pad.2.clone
  27.9 5.0 %all-to-all-done = bf16[16,128,64]{1,2,0:T(8,128)(2,1)S(1)} async-done(((bf16[16,128,64]{1,2,0:T(8,128)(2,1)}), bf16[16,128,64]{1,2,0:T(8,128)(2,1)S(1)}, u32[]{:S(2)}, u32[]{:S(2)}) %all-to-all-start) | async-done | bytes 262176 | tf_op jit(solution)/shard_map/all_to_all | solution.py:23
  33.0 0.1 fusion.34
  33.1 0.2 copy.60
  33.3 0.2 copy.61
  33.5 0.0 copy-start.2
  33.5 0.0 copy-start.3
  33.5 0.1 select_bitcast_fusion.1
  33.7 0.0 copy-start.6
  33.7 0.0 copy-start
  33.7 0.4 convolution_bitcast_fusion
  34.1 0.4 fusion.1
  34.5 0.3 convolution_bitcast_fusion.2
  34.7 0.3 fusion.2
  35.0 0.1 convolution_bitcast_fusion.5
  35.1 0.2 fusion.3
  35.3 0.2 fusion.5
  35.5 0.4 fusion.35
  35.9 0.2 multiply_reduce_fusion
  36.1 0.1 multiply_convert_fusion
  36.3 0.7 reshape.132
  37.0 10.6 %all-to-all-start.1 = ((bf16[16,2,512]{2,1,0:T(2,128)(2,1)}), bf16[16,2,512]{2,1,0:T(2,128)(2,1)S(1)}, u32[]{:S(2)}, u32[]{:S(2)}) async-start(bf16[16,2,512]{2,1,0:T(2,128)(2,1)} %reshape.132), calls=%async_computation.1 | async-start | bytes 65536 | tf_op jit(solution)/shard_map/all_to_all | solution.py:713
  47.6 0.7 maximum_maximum_fusion.table_ref
  48.2 2.4 %copy.57.gate_hbm = bf16[1,2048,448]{2,1,0:T(8,128)(2,1)} copy(bf16[1,2048,448]{1,2,0:T(8,128)(2,1)S(1)} %copy-done) | data formatting | bytes 3670016 | tf_op args[14]
  50.6 3.8 %copy.58.up_hbm = bf16[1,2048,448]{2,1,0:T(8,128)(2,1)} copy(bf16[1,2048,448]{1,2,0:T(8,128)(2,1)} %param.32) | data formatting | bytes 3670016 | tf_op args[15]
  54.5 0.5 all-to-all-done.1
  55.0 0.1 reshape.133
  55.1 0.1 all_to_all.21
  55.2 0.0 copy-start.5
  55.2 3.0 %fusion.14 = (f32[16]{0:T(128)S(1)}, bf16[16,2048]{1,0:T(8,128)(2,1)S(1)}) fusion(bf16[16,1024]{1,0:T(8,128)(2,1)S(1)} %all_to_all.21, bf16[1024,2048]{1,0:T(8,128)(2,1)} %param.26, bf16[16,2048]{1,0:T(8,128)(2,1)S(1)} %copy-done.4), kind=kOutput, calls=%fused_computation.27 | convolution fusion | flops 67305456 | bytes 4358208 | tf_op jit(solution)/shard_map/dot_general | solution.py:714
  58.2 0.7 fusion.16.normed_ref
  58.9 63.4 %shard_map.164 = bf16[16,2048]{1,0:T(8,128)(2,1)} custom-call(bf16[16,2048]{1,0:T(8,128)(2,1)} %fusion.16.normed_ref, bf16[16,2048]{1,0:T(8,128)(2,1)} %copy-done.1, f32[16,128]{1,0:T(8,128)} %maximum_maximum_fusion.table_ref, bf16[1,2048,448]{2,1,0:T(8,128)(2,1)} %copy.57.gate_hbm, bf16[1,2048,448]{2,1,0:T(8,128)(2,1)} %copy.58.up_hbm, ...), custom_call_target="tpu_custom_call" | custom-call | tf_op jit(solution)/shard_map/pallas_call | solution.py:633
  122.3 1.5 %copy.63 = bf16[16,2048]{1,0:T(8,128)(2,1)} copy(bf16[16,2048]{1,0:T(8,128)(2,1)} %shard_map.164) | data formatting | bytes 131072
  (16 shorter events, 0.1 us)
Async XLA Ops:
  17.9 15.1 %all-to-all-start = ((bf16[16,128,64]{1,2,0:T(8,128)(2,1)}), bf16[16,128,64]{1,2,0:T(8,128)(2,1)S(1)}, u32[]{:S(2)}, u32[]{:S(2)}) async-start(bf16[16,128,64]{1,2,0:T(8,128)(2,1)} %broadcast_in_dim.36), calls=%async_computation | async-start | bytes 524288 | tf_op jit(solution)/shard_map/all_to_all | solution.py:23
  33.5 2.0 %copy-start.2 = (f32[256,64]{1,0:T(8,128)S(1)}, f32[256,64]{1,0:T(8,128)}, u32[]{:S(2)}) copy-start(f32[256,64]{1,0:T(8,128)} %get-tuple-element.9) | copy-start | bytes 196612
  33.5 2.0 %copy-start.3 = (f32[256,64]{1,0:T(8,128)S(1)}, f32[256,64]{1,0:T(8,128)}, u32[]{:S(2)}) copy-start(f32[256,64]{1,0:T(8,128)} %get-tuple-element.8) | copy-start | bytes 196612
  33.7 2.4 %copy-start.6 = (f32[64]{0:T(128)S(1)}, f32[64]{0:T(128)}, u32[]{:S(2)}) copy-start(f32[64]{0:T(128)} %param.25) | copy-start | bytes 772
  33.7 14.6 %copy-start = (bf16[1,2048,448]{1,2,0:T(8,128)(2,1)S(1)}, bf16[1,2048,448]{1,2,0:T(8,128)(2,1)}, u32[]{:S(2)}) copy-start(bf16[1,2048,448]{1,2,0:T(8,128)(2,1)} %param.31) | copy-start | bytes 5505028
  37.0 18.0 %all-to-all-start.1 = ((bf16[16,2,512]{2,1,0:T(2,128)(2,1)}), bf16[16,2,512]{2,1,0:T(2,128)(2,1)S(1)}, u32[]{:S(2)}, u32[]{:S(2)}) async-start(bf16[16,2,512]{2,1,0:T(2,128)(2,1)} %reshape.132), calls=%async_computation.1 | async-start | bytes 65536 | tf_op jit(solution)/shard_map/all_to_all | solution.py:713
  50.6 4.6 %copy-start.4 = (bf16[16,2048]{1,0:T(8,128)(2,1)S(1)}, bf16[16,2048]{1,0:T(8,128)(2,1)}, u32[]{:S(2)}) copy-start(bf16[16,2048]{1,0:T(8,128)(2,1)} %param.27) | copy-start | bytes 196612
  55.2 3.0 %copy-start.5 = (f32[2048]{0:T(1024)S(1)}, f32[2048]{0:T(1024)}, u32[]{:S(2)}) copy-start(f32[2048]{0:T(1024)} %param.28) | copy-start | bytes 24580
  58.2 0.7 copy-start.1

commit v2 on v1

--- a/solution.py
+++ b/solution.py
@@ -6,79 +6,11 @@
 from jax.sharding import PartitionSpec as P
 
 HEAD_CHANNELS = 64
-TOPK = 2
-
 
 decay_factor = 0.6065306597126334
 group_eps = 0.00064
 norm_eps = 1e-06
 key_eps = 1e-06
-highest = lax.Precision.HIGHEST
-block_len = 64
-run_len = 8
-
-
-def copy_for_each(shard, axis):
-    copies = jnp.broadcast_to(shard, (lax.axis_size(axis), *shard.shape))
-    return lax.all_to_all(copies, axis, split_axis=0, concat_axis=0, tiled=True)
-
-
-def all_in_one(shard, axis):
-    leaves = jax.tree.leaves(shard)
-    order = sorted(range(len(leaves)), key=lambda k: -leaves[k].size)
-    width = (1, *leaves[order[0]].shape)[-1]
-    lines = [
-        jnp.pad(leaves[k].reshape(-1), (0, -leaves[k].size % width)).reshape(-1, width)
-        for k in order
-    ]
-    both, at, found = (copy_for_each(jnp.concatenate(lines), axis), 0, {})
-    for k, line in zip(order, lines):
-        share = both[:, at : at + len(line)].reshape(len(both), -1)
-        found[k] = share[:, : leaves[k].size].reshape(-1, *leaves[k].shape)
-        at += len(line)
-    numbers = iter(range(len(leaves)))
-    return jax.tree.map(lambda _: found[next(numbers)], shard)
-
-
-def folded_in_pairs(pieces, combine):
-    while len(jax.tree.leaves(pieces)[0]) > 1:
-        pieces = jax.vmap(combine)(
-            *(jax.tree.map(lambda part: part[side::2], pieces) for side in (0, 1))
-        )
-    return jax.tree.map(lambda part: part[0], pieces)
-
-
-def entering_2(shard, axis, combine, identity):
-    size, index = (lax.axis_size(axis), lax.axis_index(axis))
-    passed = jnp.arange(size) < index
-
-    def kept(part, zero, own):
-        part = jnp.where(
-            passed.reshape(-1, *(1 for _ in own.shape)),
-            part.astype(own.dtype),
-            jnp.asarray(zero, own.dtype),
-        )
-        return part
-
-    pieces = all_in_one(
-        jax.tree.map(
-            lambda part, kind: part.astype(kind),
-            shard,
-            jax.tree.map(lambda a: jnp.bfloat16 if a.dtype == jnp.float32 else a.dtype, shard),
-        ),
-        axis,
-    )
-    return folded_in_pairs(jax.tree.map(kept, pieces, identity, shard), combine)
-
-
-def matmul(left, right):
-    return jnp.einsum("...ij,...jk->...ik", left, right, precision=highest)
-
-
-def chain(earlier, later):
-    return (matmul(earlier[0], later[0]), matmul(earlier[1], later[0]) + later[1])
-
-
 seq_len = 256
 chunk_len = 32
 chunks = seq_len // chunk_len
@@ -116,11 +48,16 @@
     return 1.0 / (1.0 + jnp.exp(-value))
 
 
-def mixer_local(receptance, key_matrix, value_matrix, decay_input, decay_offset, head_decay, step_logits):
-    key_vec = key_matrix.astype(jnp.float32)
-    read_vec = receptance.astype(jnp.float32)
-    log_decay = head_decay - decay_factor * sigmoid(decay_input.astype(jnp.float32) + decay_offset)
-    learn = sigmoid(step_logits.astype(jnp.float32))
+def turned(value):
+    return jnp.transpose(value.astype(jnp.float32))
+
+
+def mixer_local(receptance, key_matrix, value_t, decay_input, decay_offset, head_decay, step_logits):
+    read_vec, key_vec = turned(receptance), turned(key_matrix)
+    value_matrix = turned(value_t).astype(jnp.bfloat16)
+    head_column = turned(jnp.broadcast_to(head_decay, (8, seq_len)))[:, 0:1]
+    log_decay = head_column - decay_factor * sigmoid(turned(decay_input) + decay_offset)
+    learn = turned(sigmoid(step_logits.astype(jnp.float32)))
     unit = key_vec * lax.rsqrt(jnp.sum(key_vec * key_vec, axis=1, keepdims=True) + key_eps)
     write = unit * learn
     keyed = key_vec * learn
@@ -184,7 +121,6 @@
     write_tail = jnp.where(in_block, jnp.concatenate([write * tail_scale] * chunks, axis=1), 0.0)
     keyed_tail = jnp.where(in_block, jnp.concatenate([keyed * tail_scale] * chunks, axis=1), 0.0)
     erased_t = jnp.transpose(erased)
-    value_t = jnp.transpose(value_matrix.astype(jnp.float32)).astype(jnp.bfloat16)
     maps = product(erased_t, write_tail)
     keyed_top, keyed_low = split_two(keyed_tail)
     adds = maps[64:] + dot_f32(
@@ -213,42 +149,11 @@
     return jnp.concatenate(through, axis=0), jnp.concatenate(local, axis=0), carried
 
 
-def mixer_kernel(r_ref, k_ref, v_ref, d_ref, o_ref, h_ref, c_ref, through_ref, local_ref, final_ref):
-    through, local, final = mixer_local(
-        r_ref[...], k_ref[...], v_ref[...], d_ref[...], o_ref[...], h_ref[...], c_ref[...]
-    )
-    through_ref[...] = through
-    local_ref[...] = local
-    final_ref[...] = final
-
-
-def run_mixer(*args):
-    rows = jax.ShapeDtypeStruct((seq_len, HEAD_CHANNELS), jnp.float32)
-    return pl.pallas_call(
-        mixer_kernel,
-        out_shape=(rows, rows, jax.ShapeDtypeStruct((128, 64), jnp.float32)),
-    )(*args)
-
-
-def finish(mixer_out, head_norm_scale, head_gate_rows):
-    average = jnp.mean(mixer_out, axis=-1, keepdims=True)
-    centred = mixer_out - average
-    spread = jnp.mean(centred * centred, axis=-1, keepdims=True)
-    normed = (centred * lax.rsqrt(spread + group_eps)).reshape(mixer_out.shape[0], -1)
-    return (normed * head_norm_scale[None, :] * head_gate_rows.astype(jnp.float32)).astype(
-        jnp.bfloat16
-    )
-
-
 MESH = pl.DeviceIdType.MESH
 sub_rows = 16
 subs = 4
 half = 1024
 width = 2048
-
-
-def place(axis_0, axis_1):
-    return (axis_0, axis_1)
 
 
 def transfer(source, target, send, arrive, sp, tp):
@@ -286,17 +191,64 @@
     return jnp.where(col == source_of(row), 1.0, 0.0).astype(jnp.bfloat16)
 
 
-def moe_kernel(
-    normed_ref,
-    mixed_ref,
-    table_ref,
+def fold_states(states):
+    nodes = []
+    for i in range(8):
+        early, late = states[2 * i], states[2 * i + 1]
+        stacked = jnp.concatenate([early[:, :64], early[:, 64:]], axis=0)
+        moved = dot_f32(stacked, late[:, :64])
+        nodes.append((moved[:64], moved[64:] + late[:, 64:].astype(jnp.float32)))
+    while len(nodes) > 1:
+        joined = []
+        for i in range(0, len(nodes), 2):
+            (early_map, early_state), (late_map, late_state) = nodes[i], nodes[i + 1]
+            if i == 0:
+                joined.append((None, product(early_state, late_map) + late_state))
+            else:
+                moved = product(jnp.concatenate([early_map, early_state], axis=0), late_map)
+                joined.append((moved[:64], moved[64:] + late_state))
+        nodes = joined
+    return nodes[0][1]
+
+
+def finish(mixer_out, head_norm_scale, head_gate_rows):
+    average = jnp.mean(mixer_out, axis=1, keepdims=True)
+    centred = mixer_out - average
+    spread = jnp.mean(centred * centred, axis=1, keepdims=True)
+    return centred * lax.rsqrt(spread + group_eps) * head_norm_scale * head_gate_rows
+
+
+def layer_kernel(
+    r_ref,
+    k_ref,
+    v_ref,
+    d_ref,
+    o_ref,
+    h_ref,
+    c_ref,
+    g_ref,
+    scale_ref,
+    residual_ref,
+    norm_ref,
+    index_ref,
+    score_ref,
+    mix_hbm,
     gate_hbm,
     up_hbm,
     down_hbm,
     out_ref,
+    mix_mat,
     gate_mat,
     up_mat,
     down_mat,
+    through_ref,
+    local_ref,
+    state_out,
+    states,
+    heads_out,
+    heads_in,
+    mixed_ref,
+    table_ref,
     outgoing,
     incoming,
     tables,
@@ -312,6 +264,10 @@
     sent_sum,
     got_sum,
     weight_sem,
+    state_send,
+    state_recv,
+    heads_send,
+    heads_recv,
     table_send,
     table_recv,
     spread_send,
@@ -332,52 +288,157 @@
     twin = level * 2 + (1 - core)
 
     loads = [
-        pltpu.make_async_copy(source.at[0], target, weight_sem.at[k])
+        pltpu.make_async_copy(source, target, weight_sem.at[k])
         for k, (source, target) in enumerate(
-            ((gate_hbm, gate_mat), (up_hbm, up_mat), (down_hbm, down_mat))
+            (
+                (mix_hbm, mix_mat),
+                (gate_hbm.at[0], gate_mat),
+                (up_hbm.at[0], up_mat),
+                (down_hbm.at[0], down_mat),
+            )
         )
     ]
     for load in loads:
         load.start()
 
+    start_row = lax.broadcasted_iota(jnp.int32, (16, 64, 128), 1)
+    start_col = lax.broadcasted_iota(jnp.int32, (16, 64, 128), 2)
+    states[...] = jnp.where(start_row == start_col, 1.0, 0.0).astype(jnp.bfloat16)
+
     barrier = pltpu.get_barrier_semaphore()
     for j in range(1, 16):
         pl.semaphore_signal(barrier, inc=1, device_id=((sp + j) % 16, tp), device_id_type=MESH)
         pl.semaphore_signal(barrier, inc=1, device_id=(sp, (tp + j) % 16), device_id_type=MESH)
 
-    own_table = table_ref[...]
-    first, second = ranks_of(own_table[:, 0:1], own_table[:, 1:2])
-    lane = lax.broadcasted_iota(jnp.int32, (16, 256), 1).astype(jnp.float32)
-    spread = jnp.concatenate(
+    through, local, final = mixer_local(
+        r_ref[...], k_ref[...], v_ref[...], d_ref[...], o_ref[...], h_ref[...], c_ref[...]
+    )
+    state_out[...] = jnp.concatenate([final[:64], final[64:]], axis=1).astype(jnp.bfloat16)
+    through_ref[...] = through
+    local_ref[...] = local
+    table_ref[...] = jnp.concatenate(
         [
-            jnp.where((lane == first + 4.0 * q) | (lane == second + 4.0 * q), 1.0, 0.0)
-            for q in range(4)
+            jnp.transpose(
+                jnp.concatenate(
+                    [
+                        jnp.concatenate(
+                            [index_ref[...].astype(jnp.float32), score_ref[...]], axis=0
+                        ),
+                        jnp.zeros((4, 112), jnp.float32),
+                    ],
+                    axis=1,
+                )
+            )[:16],
+            jnp.zeros((16, 124), jnp.float32),
         ],
-        axis=0,
-    )
-    normed = normed_ref[...]
-    stacked = jnp.concatenate([normed[:, q * 512 : (q + 1) * 512] for q in range(4)], axis=0)
-    outgoing[...] = dot_f32(
-        jnp.transpose(spread).astype(jnp.bfloat16), stacked
-    ).astype(jnp.bfloat16).reshape(16, 16, 512)
+        axis=1,
+    )
 
     pl.semaphore_wait(barrier, 30)
 
     pending = []
-    for j in range(1, 16):
-        other = (sp + j) % 16
-        copy = transfer(
-            outgoing.at[other], incoming.at[sp], spread_send.at[j], spread_recv.at[sp], other, tp
-        )
-        copy.start()
-        pending.append(copy)
-    incoming[sp] = outgoing[sp]
+
+    def state_copy(j, source, target):
+        return transfer(
+            state_out, states.at[source], state_send.at[j], state_recv.at[source], target, tp
+        )
+
+    for j in range(1, 16):
+
+        @pl.when(sp + j < 16)
+        def _():
+            state_copy(j, sp, sp + j).start()
+
     for j in range(1, 16):
         other = (tp + j) % 16
         copy = transfer(table_ref, tables.at[tp], table_send.at[j], table_recv.at[tp], sp, other)
         copy.start()
         pending.append(copy)
-    tables[tp] = own_table
+    tables[tp] = table_ref[...]
+
+    own_table = table_ref[...]
+    first, second = ranks_of(own_table[:, 0:1], own_table[:, 1:2])
+    lane = lax.broadcasted_iota(jnp.int32, (16, 256), 1).astype(jnp.float32)
+    spread = jnp.transpose(
+        jnp.concatenate(
+            [
+                jnp.where((lane == first + 4.0 * q) | (lane == second + 4.0 * q), 1.0, 0.0)
+                for q in range(4)
+            ],
+            axis=0,
+        )
+    ).astype(jnp.bfloat16)
+
+    for j in range(1, 16):
+
+        @pl.when(sp - j >= 0)
+        def _():
+            state_copy(j, sp - j, sp).wait_recv()
+
+    entering = fold_states(states[...])
+    attended = finish(
+        local_ref[...] + product_nt(through_ref[...], entering), scale_ref[...], turned(g_ref[...])
+    )
+    both = jnp.concatenate([attended, attended], axis=1)
+    side_lane = lax.broadcasted_iota(jnp.int32, (seq_len, 128), 1) // 64
+    heads_out[...] = jnp.where(side_lane == core, both, 0.0).astype(jnp.bfloat16).reshape(16, 16, 128)
+    for j in range(1, 16):
+        other = (tp + j) % 16
+        copy = transfer(
+            heads_out.at[other], heads_in.at[tp], heads_send.at[j], heads_recv.at[tp], sp, other
+        )
+        copy.start()
+        pending.append(copy)
+    heads_in[tp] = heads_out[tp]
+
+    for j in range(1, 16):
+        other = (tp + j) % 16
+        transfer(
+            table_ref, tables.at[other], table_send.at[j], table_recv.at[other], sp, other
+        ).wait_recv()
+    every = tables[...].reshape(256, 128)
+    all_first, all_second = ranks_of(every[:, 0:1], every[:, 1:2])
+    gap = every[:, 3:4] - every[:, 2:3]
+    wide_lane = lax.broadcasted_iota(jnp.int32, (256, 128), 1)
+    codes[...] = jnp.where(
+        wide_lane == 0,
+        all_first,
+        jnp.where(
+            wide_lane == 1,
+            all_second,
+            jnp.where(wide_lane == 2, 1.0 / (1.0 + jnp.exp(gap)), 1.0 / (1.0 + jnp.exp(-gap))),
+        ),
+    ).reshape(16, 16, 128)
+    for load in loads:
+        load.wait()
+
+    for j in range(1, 16):
+        other = (tp + j) % 16
+        transfer(
+            heads_out.at[other], heads_in.at[other], heads_send.at[j], heads_recv.at[other], sp, other
+        ).wait_recv()
+    tokens = jnp.concatenate([heads_in[2 * i] + heads_in[2 * i + 1] for i in range(8)], axis=1)
+    mixed_f = (
+        (residual_ref[...].astype(jnp.float32) + dot_f32(tokens, mix_mat[...]))
+        .astype(jnp.bfloat16)
+        .astype(jnp.float32)
+    )
+    mixed_ref[...] = mixed_f
+    normed = (
+        mixed_f
+        * lax.rsqrt(jnp.mean(mixed_f * mixed_f, axis=1, keepdims=True) + norm_eps)
+        * norm_ref[...]
+    ).astype(jnp.bfloat16)
+    stacked = jnp.concatenate([normed[:, q * 512 : (q + 1) * 512] for q in range(4)], axis=0)
+    outgoing[...] = dot_f32(spread, stacked).astype(jnp.bfloat16).reshape(16, 16, 512)
+    for j in range(1, 16):
+        other = (sp + j) % 16
+        copy = transfer(
+            outgoing.at[other], incoming.at[sp], spread_send.at[j], spread_recv.at[sp], other, tp
+        )
+        copy.start()
+        pending.append(copy)
+    incoming[sp] = outgoing[sp]
 
     for j in range(1, 16):
         other = (sp + j) % 16
@@ -463,27 +524,6 @@
         high = block_at(distance, 1) * 2
         return (low, low + 1, high, high + 1)
 
-    for j in range(1, 16):
-        other = (tp + j) % 16
-        transfer(
-            table_ref, tables.at[other], table_send.at[j], table_recv.at[other], sp, other
-        ).wait_recv()
-    every = tables[...].reshape(256, 128)
-    first, second = ranks_of(every[:, 0:1], every[:, 1:2])
-    gap = every[:, 3:4] - every[:, 2:3]
-    wide_lane = lax.broadcasted_iota(jnp.int32, (256, 128), 1)
-    codes[...] = jnp.where(
-        wide_lane == 0,
-        first,
-        jnp.where(
-            wide_lane == 1,
-            second,
-            jnp.where(wide_lane == 2, 1.0 / (1.0 + jnp.exp(gap)), 1.0 / (1.0 + jnp.exp(-gap))),
-        ),
-    ).reshape(16, 16, 128)
-    for load in loads:
-        load.wait()
-
     reorder = one_hot_rows(lambda j: ((j >> 2) & 3) * 64 + (j >> 4) * 4 + (j & 3))
     core_at = pl.multiple_of(core * half, half)
     twin_at = pl.multiple_of((1 - core) * half, half)
@@ -492,10 +532,10 @@
         return jnp.concatenate([rows_all[index] for index in members(distance)], axis=0)
 
     def stage_gate(distance):
-        gate_act[...] = dot_f32(rows_in(distance), gate_mat[...])
+        gate_act[...] = dot_f32(rows_in(distance), gate_mat[...], (((1,), (1,)), ((), ())))
 
     def stage_up(distance):
-        up_act = dot_f32(rows_in(distance), up_mat[...])
+        up_act = dot_f32(rows_in(distance), up_mat[...], (((1,), (1,)), ((), ())))
         gate = gate_act[...]
         hidden = (gate / (1.0 + jnp.exp(-gate)) * up_act).astype(jnp.bfloat16)
         hidden_rows[...] = dot_f32(reorder, hidden).astype(jnp.bfloat16)
@@ -621,58 +661,14 @@
         for stage in range(1, 8):
             gathered = gathered + got_sum[2 * stage + side].astype(jnp.float32)
         cut = slice(side * half, (side + 1) * half)
-        out_ref[:, cut] = (mixed_ref[:, cut].astype(jnp.float32) + gathered).astype(jnp.bfloat16)
+        out_ref[:, cut] = (mixed_ref[:, cut] + gathered).astype(jnp.bfloat16)
     for copy in pending:
         copy.wait_send()
-
-
-def run_moe(normed, mixed, table, gate, up, down):
-    vmem = pl.BlockSpec(memory_space=pltpu.VMEM)
-    hbm = pl.BlockSpec(memory_space=pl.ANY)
-    dma = pltpu.SemaphoreType.DMA
-    return pl.pallas_call(
-        moe_kernel,
-        out_shape=jax.ShapeDtypeStruct((16, width), jnp.bfloat16),
-        in_specs=[vmem, vmem, vmem, hbm, hbm, hbm],
-        out_specs=vmem,
-        scratch_shapes=[
-            pltpu.VMEM((width, 448), jnp.bfloat16),
-            pltpu.VMEM((width, 448), jnp.bfloat16),
-            pltpu.VMEM((448, width), jnp.bfloat16),
-            pltpu.VMEM((16, 16, 512), jnp.bfloat16),
-            pltpu.VMEM((16, 16, 512), jnp.bfloat16),
-            pltpu.VMEM((16, 16, 128), jnp.float32),
-            pltpu.VMEM((16, 16, 128), jnp.float32),
-            pltpu.VMEM((16, 64, width), jnp.bfloat16),
-            pltpu.VMEM((256, 448), jnp.float32),
-            pltpu.VMEM((256, 448), jnp.bfloat16),
-            pltpu.VMEM((256, half), jnp.float32),
-            pltpu.VMEM((4, 256, half), jnp.bfloat16),
-            pltpu.VMEM((4, 256, half), jnp.bfloat16),
-            pltpu.VMEM((4, 16, 16, half), jnp.bfloat16),
-            pltpu.VMEM((4, 16, 16, half), jnp.bfloat16),
-            pltpu.VMEM((4, 4, 16, half), jnp.bfloat16),
-            pltpu.VMEM((16, 16, half), jnp.bfloat16),
-            dma((3,)),
-            dma((16,)),
-            dma((16,)),
-            dma((16,)),
-            dma((16,)),
-            dma((2, 14)),
-            dma((2, 14)),
-            dma((32,)),
-            dma((32,)),
-            dma((4,)),
-            dma((4,)),
-            dma((4, 16)),
-            dma((4, 16)),
-            dma((4, 4)),
-            dma((16,)),
-        ],
-        compiler_params=pltpu.CompilerParams(
-            collective_id=1, has_side_effects=True, vmem_limit_bytes=56 * 1024 * 1024
-        ),
-    )(normed, mixed, table, gate, up, down)
+    for j in range(1, 16):
+
+        @pl.when(sp + j < 16)
+        def _():
+            state_copy(j, sp, sp + j).wait_send()
 
 
 def shards(
@@ -694,40 +690,72 @@
     expert_up_weight,
     expert_down_weight,
 ):
-    through, local_out, final = run_mixer(
-        receptance,
-        key_matrix,
-        value_matrix,
-        decay_input_term,
+    vmem = pl.BlockSpec(memory_space=pltpu.VMEM)
+    hbm = pl.BlockSpec(memory_space=pl.ANY)
+    dma = pltpu.SemaphoreType.DMA
+    b16, f32 = jnp.bfloat16, jnp.float32
+    return pl.pallas_call(
+        layer_kernel,
+        out_shape=jax.ShapeDtypeStruct((16, width), jnp.bfloat16),
+        in_specs=[vmem] * 13 + [hbm] * 4,
+        out_specs=vmem,
+        scratch_shapes=[
+            pltpu.VMEM((1024, width), b16),
+            pltpu.VMEM((448, width), b16),
+            pltpu.VMEM((448, width), b16),
+            pltpu.VMEM((448, width), b16),
+            pltpu.VMEM((seq_len, 64), f32),
+            pltpu.VMEM((seq_len, 64), f32),
+            pltpu.VMEM((64, 128), b16),
+            pltpu.VMEM((16, 64, 128), b16),
+            pltpu.VMEM((16, 16, 128), b16),
+            pltpu.VMEM((16, 16, 128), b16),
+            pltpu.VMEM((16, width), f32),
+            pltpu.VMEM((16, 128), f32),
+            pltpu.VMEM((16, 16, 512), b16),
+            pltpu.VMEM((16, 16, 512), b16),
+            pltpu.VMEM((16, 16, 128), f32),
+            pltpu.VMEM((16, 16, 128), f32),
+            pltpu.VMEM((16, 64, width), b16),
+            pltpu.VMEM((256, 448), f32),
+            pltpu.VMEM((256, 448), b16),
+            pltpu.VMEM((256, half), f32),
+            pltpu.VMEM((4, 256, half), b16),
+            pltpu.VMEM((4, 256, half), b16),
+            pltpu.VMEM((4, 16, 16, half), b16),
+            pltpu.VMEM((4, 16, 16, half), b16),
+            pltpu.VMEM((4, 4, 16, half), b16),
+            pltpu.VMEM((16, 16, half), b16),
+            dma((4,)),
+        ]
+        + [dma((16,))] * 8
+        + [dma((2, 14))] * 2
+        + [dma((32,))] * 2
+        + [dma((4,))] * 2
+        + [dma((4, 16))] * 2
+        + [dma((4, 4)), dma((16,))],
+        compiler_params=pltpu.CompilerParams(
+            collective_id=1, has_side_effects=True, vmem_limit_bytes=56 * 1024 * 1024
+        ),
+    )(
+        receptance.T,
+        key_matrix.T,
+        value_matrix.T,
+        decay_input_term.T,
         decay_channel_offset.reshape(1, -1),
-        head_log_decay,
-        context_step_logits,
-    )
-    through, local_out = through[:, None, :], local_out[:, None, :]
-    final = (final[None, :64], final[None, 64:])
-    start_map = jnp.broadcast_to(jnp.eye(final[0].shape[1], dtype=jnp.float32), final[0].shape)
-    entering = entering_2(final, "sp", chain, (start_map, jnp.zeros_like(final[1])))
-    mixer_out = local_out + jnp.einsum("hij,thj->thi", entering[1], through, precision=highest)
-    attended = finish(mixer_out, head_norm_scale, head_gate_rows)
-    row_count = residual.shape[0]
-    token_rows = lax.all_to_all(attended, "tp", split_axis=0, concat_axis=1, tiled=True)
-    projected = jnp.dot(token_rows, mixer_output_weight, preferred_element_type=jnp.float32)
-    mixed = (residual.astype(jnp.float32) + projected).astype(jnp.bfloat16)
-    mixed_f = mixed.astype(jnp.float32)
-    normed = (
-        mixed_f
-        * lax.rsqrt(jnp.mean(mixed_f * mixed_f, axis=-1, keepdims=True) + norm_eps)
-        * expert_norm_scale[None, :]
-    ).astype(jnp.bfloat16)
-    table = jnp.concatenate(
-        [
-            expert_index_table.astype(jnp.float32),
-            expert_router_scores,
-            jnp.zeros((row_count, 124), jnp.float32),
-        ],
-        axis=1,
-    )
-    return run_moe(normed, mixed, table, expert_gate_weight, expert_up_weight, expert_down_weight)
+        head_log_decay.T,
+        context_step_logits.T,
+        head_gate_rows.T,
+        head_norm_scale.reshape(1, -1),
+        residual,
+        expert_norm_scale.reshape(1, -1),
+        expert_index_table.T,
+        expert_router_scores.T,
+        mixer_output_weight,
+        jnp.swapaxes(expert_gate_weight, 1, 2),
+        jnp.swapaxes(expert_up_weight, 1, 2),
+        expert_down_weight,
+    )
 
 
 def solution(mesh):

time: 125 us -> 86.9 us (0.70)
  local copies, waits for them, and re-layouts: 20.7 us -> 1.47 us
  starting transfers between devices: 18.2 us -> 0 us
  Pallas kernels: 70.7 us -> 85.3 us
  waiting for transfers between devices: 5.53 us -> 0 us
  matrix products: 5.1 us -> 0 us
  other arithmetic: 3.4 us -> 0 us
    all_to_all x2 -> x0, starting transfers between devices: 18.2 us -> none  [the longest x1 10.6 us: shards(): lax.all_to_all(attended, 'tp', split_axis=0, concat_axis=1, tiled=True)]
    unnamed x29 -> x1, local copies, waits for them, and re-layouts: 19.4 us -> 1.47 us
    pallas_call x2 -> x1, Pallas kernels: 70.7 us -> 85.3 us  [shards(): pl.pallas_call(layer_kernel, out_shape=jax.ShapeDtypeStruct((16, width),...]
    all_to_all x2 -> x0, waiting for transfers between devices: 5.53 us -> none  [the longest x1 5.04 us: copy_for_each(): return lax.all_to_all(copies, axis, split_axis=0, concat_axis=0, tiled=True)]
    dot_general x8 -> x0, matrix products: 4.96 us -> none  [the longest x1 2.96 us: shards(): jnp.dot(token_rows, mixer_output_weight, preferred_element_type=jnp.float32)]
    convert_element_type x4 -> x0, other arithmetic: 1.54 us -> none  [the longest x1 0.71 us: shards(): normed = (mixed_f * lax.rsqrt(jnp.mean(mixed_f * mixed_f, axis=-1, keepdi...]
  transfers between devices with their start and end apart: 2 -> 0, of which waited for: 2 -> 0; matrix products, arithmetic and copies ran while one was open for 8% -> 0% of each run, Pallas kernels for 0% -> 0%
where the time goes in v2:
time: 86.9 us; the launch traced here: 86.8 us
  Pallas kernels  85.3 us (98%)
  local copies, waits for them, and re-layouts  1.47 us (2%)
    pallas_call x1, Pallas kernels, shards(): pl.pallas_call(layer_kernel, out_shape=jax.ShapeDtypeStruct((16, width),...  85.3 us

profile of v2, /device:TPU:1, one launch (start us, length us, event | category | flops | bytes accessed | tf_op | source)
XLA Modules:
  0.0 86.8 jit_solution(771474509590806803)
XLA Ops:
  0.0 85.3 %shard_map.163 = bf16[16,2048]{1,0:T(8,128)(2,1)} custom-call(bf16[64,256]{1,0:T(8,128)(2,1)} %bitcast.16, bf16[64,256]{1,0:T(8,128)(2,1)} %bitcast.17, bf16[64,256]{1,0:T(8,128)(2,1)} %bitcast.18, bf16[64,256]{1,0:T(8,128)(2,1)} %bitcast.19, f32[1,64]{1,0:T(1,128)} %bitcast.26, f32[1,256]{1,0:T(1,128)} %bitcast.23, bf16[64,256]{1,0:T(8,128)(2,1)} %bitcast.20, ...), custom_call_target="tpu_custom_call" | custom-call | tf_op jit(solution)/shard_map/pallas_call | solution.py:697
  85.3 1.5 %copy.19 = bf16[16,2048]{1,0:T(8,128)(2,1)} copy(bf16[16,2048]{1,0:T(8,128)(2,1)} %shard_map.163) | data formatting | bytes 131072

commit v3 on v2

v3 whole, which is shorter than its diff:
```python
import jax
import jax.numpy as jnp
from jax import lax
from jax.experimental import pallas as pl
from jax.experimental.pallas import tpu as pltpu
from jax.sharding import PartitionSpec as P

HEAD_CHANNELS = 64

decay_factor = 0.6065306597126334
group_eps = 0.00064
norm_eps = 1e-06
key_eps = 1e-06
seq_len = 256
chunk_len = 32
chunks = seq_len // chunk_len


def split_two(value):
    top = value.astype(jnp.bfloat16)
    return top, (value - top.astype(jnp.float32)).astype(jnp.bfloat16)


def dot_f32(left, right, dims=(((1,), (0,)), ((), ()))):
    return lax.dot_general(left, right, dims, preferred_element_type=jnp.float32)


def product(left, right):
    left_top, left_low = split_two(left)
    right_top, right_low = split_two(right)
    return dot_f32(
        jnp.concatenate([left_top, left_top, left_low], axis=1),
        jnp.concatenate([right_top, right_low, right_top], axis=0),
    )


def product_nt(left, right):
    left_top, left_low = split_two(left)
    right_top, right_low = split_two(right)
    return dot_f32(
        jnp.concatenate([left_top, left_top, left_low], axis=1),
        jnp.concatenate([right_top, right_low, right_top], axis=1),
        (((1,), (1,)), ((), ())),
    )


def sigmoid(value):
    return 1.0 / (1.0 + jnp.exp(-value))


def turned(value):
    return jnp.transpose(value.astype(jnp.float32))


def mixer_local(receptance, key_matrix, value_t, decay_input, decay_offset, head_decay, step_logits):
    read_vec, key_vec = turned(receptance), turned(key_matrix)
    value_matrix = turned(value_t).astype(jnp.bfloat16)
    head_column = turned(jnp.broadcast_to(head_decay, (8, seq_len)))[:, 0:1]
    log_decay = head_column - decay_factor * sigmoid(turned(decay_input) + decay_offset)
    learn = turned(sigmoid(step_logits.astype(jnp.float32)))
    unit = key_vec * lax.rsqrt(jnp.sum(key_vec * key_vec, axis=1, keepdims=True) + key_eps)
    write = unit * learn
    keyed = key_vec * learn

    row = lax.broadcasted_iota(jnp.int32, (seq_len, seq_len), 0)
    col = lax.broadcasted_iota(jnp.int32, (seq_len, seq_len), 1)
    same = (row >> 5) == (col >> 5)
    upto = same & (col <= row)
    before = same & (col < row)

    log_top, log_rest = split_two(log_decay)
    log_low = (log_decay - log_top.astype(jnp.float32) - log_rest.astype(jnp.float32)).astype(jnp.bfloat16)
    summed = dot_f32(
        jnp.where(upto, 1.0, 0.0).astype(jnp.bfloat16),
        jnp.concatenate([log_top, log_rest, log_low], axis=1),
    )
    total = summed[:, :64] + summed[:, 64:128] + summed[:, 128:192]
    by_chunk = total.reshape(chunks, chunk_len, HEAD_CHANNELS)
    middle = jnp.broadcast_to(by_chunk[:, chunk_len // 2 - 1 : chunk_len // 2], by_chunk.shape).reshape(total.shape)
    last = by_chunk[:, chunk_len - 1 : chunk_len]
    ending = jnp.broadcast_to(last, by_chunk.shape).reshape(total.shape)
    prior = total - log_decay

    up_scale = jnp.exp(middle - total)
    scaled = jnp.concatenate([write * up_scale, keyed * up_scale], axis=0)
    gram = product_nt(-unit * jnp.exp(prior - middle), scaled)
    erase_write = jnp.where(before, gram[:, :seq_len], 0.0)
    erase_keyed = jnp.where(before, gram[:, seq_len:], 0.0)

    def below(width):
        return (
            ((row & (-2 * width)) == (col & (-2 * width)))
            & ((row & width) != 0)
            & ((col & width) == 0)
        )

    solved = jnp.where(row == col, 1.0, 0.0) + jnp.where(below(1), erase_write, 0.0)
    for width in (2, 4, 8, 16):
        solved = solved + product(solved, product(jnp.where(below(width), erase_write, 0.0), solved))

    def on_values(weights):
        top, low = split_two(weights)
        return dot_f32(
            jnp.concatenate([top, low], axis=1),
            jnp.concatenate([value_matrix, value_matrix], axis=0),
        )

    erased = product(
        solved, jnp.concatenate([-unit * jnp.exp(prior), on_values(erase_keyed)], axis=1)
    )
    tail_scale = jnp.exp(ending - total)
    wide_row = lax.broadcasted_iota(jnp.int32, (seq_len, chunks * 64), 0)
    wide_col = lax.broadcasted_iota(jnp.int32, (seq_len, chunks * 64), 1)
    in_block = (wide_row >> 5) == (wide_col >> 6)
    write_tail = jnp.where(in_block, jnp.concatenate([write * tail_scale] * chunks, axis=1), 0.0)
    keyed_tail = jnp.where(in_block, jnp.concatenate([keyed * tail_scale] * chunks, axis=1), 0.0)
    erased_t = jnp.transpose(erased)
    maps = product(erased_t, write_tail)
    keyed_top, keyed_low = split_two(keyed_tail)
    adds = maps[64:] + dot_f32(
        jnp.concatenate([value_t, value_t], axis=1),
        jnp.concatenate([keyed_top, keyed_low], axis=0),
    )
    small_row = lax.broadcasted_iota(jnp.int32, (64, 64), 0)
    small_col = lax.broadcasted_iota(jnp.int32, (64, 64), 1)
    eye = small_row == small_col

    def joined(early, late):
        moved = product(early, late[:64])
        return jnp.concatenate([moved[:64], moved[64:] + late[64:]], axis=0)

    steps = []
    for c in range(chunks):
        step_map = maps[:64, c * 64 : (c + 1) * 64] + jnp.where(eye, jnp.exp(last[c]), 0.0)
        steps.append(jnp.concatenate([step_map, adds[:, c * 64 : (c + 1) * 64]], axis=0))
    pairs = [joined(steps[2 * i], steps[2 * i + 1]) for i in range(4)]
    quads = [joined(pairs[0], pairs[1]), joined(pairs[2], pairs[3])]

    def outputs():
        gram_read = product_nt(read_vec * jnp.exp(total - middle), scaled)
        read_write = jnp.where(upto, gram_read[:, :seq_len], 0.0)
        read_keyed = jnp.where(upto, gram_read[:, seq_len:], 0.0)
        shown = product(read_write, erased)
        seen = read_vec * jnp.exp(total) + shown[:, :64]
        own = shown[:, 64:] + on_values(read_keyed)
        six = joined(quads[0], pairs[2])
        entering = (
            steps[0],
            pairs[0],
            joined(pairs[0], steps[2]),
            quads[0],
            joined(quads[0], steps[4]),
            six,
            joined(six, steps[6]),
        )
        through = [seen[:chunk_len]]
        local = [own[:chunk_len]]
        for c in range(1, chunks):
            part = slice(c * chunk_len, (c + 1) * chunk_len)
            viewed = product_nt(seen[part], entering[c - 1])
            through.append(viewed[:, :64])
            local.append(viewed[:, 64:] + own[part])
        return jnp.concatenate(through, axis=0), jnp.concatenate(local, axis=0)

    return joined(quads[0], quads[1]), outputs


MESH = pl.DeviceIdType.MESH
sub_rows = 16
subs = 4
half = 1024
width = 2048


def transfer(source, target, send, arrive, sp, tp):
    return pltpu.make_async_remote_copy(
        src_ref=source,
        dst_ref=target,
        send_sem=send,
        recv_sem=arrive,
        device_id=(sp, tp),
        device_id_type=MESH,
    )


def settle(block, sem):
    pltpu.make_async_copy(block, block, sem).wait()


def split_three(value):
    top, low = split_two(value)
    return top, low, (value - top.astype(jnp.float32) - low.astype(jnp.float32)).astype(jnp.bfloat16)


def ranks_of(first, second):
    count = first.shape[0]
    lane = lax.broadcasted_iota(jnp.int32, (count, 128), 1).astype(jnp.float32)
    hit_0 = jnp.where(lane == first, 1.0, 0.0)
    hit_1 = jnp.where(lane == second, 1.0, 0.0)
    row = lax.broadcasted_iota(jnp.int32, (count, count), 0)
    col = lax.broadcasted_iota(jnp.int32, (count, count), 1)
    same = (row >> 4) == (col >> 4)
    earlier = dot_f32(
        jnp.where(same & (col < row), 1.0, 0.0).astype(jnp.bfloat16),
        jnp.concatenate([hit_0, hit_1], axis=1).astype(jnp.bfloat16),
    )
    every = dot_f32(jnp.where(same, 1.0, 0.0).astype(jnp.bfloat16), hit_0.astype(jnp.bfloat16))
    rank_0 = jnp.sum(earlier[:, :128] * hit_0, axis=1, keepdims=True)
    rank_1 = jnp.sum((earlier[:, 128:] + every) * hit_1, axis=1, keepdims=True)
    return rank_0, rank_1


def fold_states(states):
    nodes = []
    for i in range(8):
        early, late = states[2 * i], states[2 * i + 1]
        stacked = jnp.concatenate([early[:, :64], early[:, 64:]], axis=0)
        moved = dot_f32(stacked, late[:, :64])
        nodes.append((moved[:64], moved[64:] + late[:, 64:].astype(jnp.float32)))
    while len(nodes) > 1:
        joined = []
        for i in range(0, len(nodes), 2):
            (early_map, early_state), (late_map, late_state) = nodes[i], nodes[i + 1]
            if i == 0:
                joined.append((None, product(early_state, late_map) + late_state))
            else:
                moved = product(jnp.concatenate([early_map, early_state], axis=0), late_map)
                joined.append((moved[:64], moved[64:] + late_state))
        nodes = joined
    return nodes[0][1]


def finish(mixer_out, head_norm_scale, head_gate_rows):
    average = jnp.mean(mixer_out, axis=1, keepdims=True)
    centred = mixer_out - average
    spread = jnp.mean(centred * centred, axis=1, keepdims=True)
    return centred * lax.rsqrt(spread + group_eps) * head_norm_scale * head_gate_rows


def layer_kernel(
    r_ref,
    k_ref,
    v_ref,
    d_ref,
    o_ref,
    h_ref,
    c_ref,
    g_ref,
    scale_ref,
    residual_ref,
    norm_ref,
    index_ref,
    score_ref,
    mix_hbm,
    gate_hbm,
    up_hbm,
    down_hbm,
    out_ref,
    mix_mat,
    gate_mat,
    up_mat,
    down_mat,
    gate_nat,
    up_nat,
    through_ref,
    local_ref,
    state_out,
    states,
    heads_out,
    heads_in,
    mixed_ref,
    table_ref,
    outgoing,
    incoming,
    codes,
    rows_all,
    gate_act,
    hidden_rows,
    mine_part,
    pair_out,
    pair_in,
    leave,
    back,
    sent_sum,
    pair_out_s,
    pair_in_s,
    leave_s,
    back_s,
    sent_sum_s,
    got_sum,
    weight_sem,
    state_send,
    state_recv,
    single_sem,
    spread_recv,
    ring_recv,
    twin_recv,
    pair_send,
    pair_recv,
    back_send,
    back_recv,
):
    sp, tp = lax.axis_index("sp"), lax.axis_index("tp")
    level, core = tp // 2, tp % 2
    twin = level * 2 + (1 - core)
    heads_send, heads_recv, spread_send, ring_send, twin_send, sum_send, sum_recv = (
        single_sem.at[k] for k in range(7)
    )

    loads = [
        pltpu.make_async_copy(source, target, weight_sem.at[k])
        for k, (source, target) in enumerate(
            (
                (mix_hbm, mix_mat),
                (gate_hbm.at[0], gate_mat),
                (up_hbm.at[0], up_mat),
                (down_hbm.at[0], down_mat),
            )
        )
    ]
    for load in loads:
        load.start()

    start_row = lax.broadcasted_iota(jnp.int32, (16, 64, 128), 1)
    start_col = lax.broadcasted_iota(jnp.int32, (16, 64, 128), 2)
    states[...] = jnp.where(start_row == start_col, 1.0, 0.0).astype(jnp.bfloat16)

    barrier = pltpu.get_barrier_semaphore()
    for j in range(1, 16):
        pl.semaphore_signal(barrier, inc=1, device_id=((sp + j) % 16, tp), device_id_type=MESH)
        pl.semaphore_signal(barrier, inc=1, device_id=(sp, (tp + j) % 16), device_id_type=MESH)

    final, outputs = mixer_local(
        r_ref[...], k_ref[...], v_ref[...], d_ref[...], o_ref[...], h_ref[...], c_ref[...]
    )
    state_out[...] = jnp.concatenate([final[:64], final[64:]], axis=1).astype(jnp.bfloat16)
    own_table = jnp.transpose(
        jnp.concatenate(
            [
                jnp.concatenate([index_ref[...].astype(jnp.float32), score_ref[...]], axis=0),
                jnp.zeros((4, 112), jnp.float32),
            ],
            axis=1,
        )
    )[:16]
    table_ref[...] = own_table

    pl.semaphore_wait(barrier, 30)

    def state_copy(j, source, target):
        return transfer(
            state_out, states.at[source], state_send.at[j], state_recv.at[source], target, tp
        )

    for j in range(1, 16):

        @pl.when(sp + j < 16)
        def _():
            state_copy(j, sp, sp + j).start()

    through_ref[...], local_ref[...] = outputs()

    own_table = table_ref[...]
    rank_0, rank_1 = ranks_of(own_table[:, 0:1], own_table[:, 1:2])
    first, second = own_table[:, 0:1] * 16.0 + rank_0, own_table[:, 1:2] * 16.0 + rank_1
    lane = lax.broadcasted_iota(jnp.int32, (16, 256), 1).astype(jnp.float32)
    spread = jnp.transpose(
        jnp.concatenate(
            [
                jnp.where((lane == first + 4.0 * q) | (lane == second + 4.0 * q), 1.0, 0.0)
                for q in range(4)
            ],
            axis=0,
        )
    ).astype(jnp.bfloat16)

    for j in range(1, 16):

        @pl.when(sp - j >= 0)
        def _():
            state_copy(j, sp - j, sp).wait_recv()

    entering = fold_states(states[...])
    attended = finish(
        local_ref[...] + product_nt(through_ref[...], entering), scale_ref[...], turned(g_ref[...])
    )
    score_parts = [
        part for k in (2, 3) for part in split_three(own_table[:, k : k + 1])
    ]
    notes = jnp.concatenate(
        [own_table[:, 0:2].astype(jnp.bfloat16)] + score_parts + [jnp.zeros((16, 56), jnp.bfloat16)],
        axis=1,
    ).astype(jnp.float32)
    notes = jnp.broadcast_to(
        jnp.concatenate([notes, notes], axis=1)[None], (16, 16, 128)
    )
    both = jnp.concatenate([attended, attended], axis=1).reshape(16, 16, 128)
    side_lane = lax.broadcasted_iota(jnp.int32, (16, 16, 128), 2) // 64
    heads_out[...] = jnp.where(side_lane == core, both, notes).astype(jnp.bfloat16)
    for j in range(1, 16):
        other = (tp + j) % 16
        transfer(
            heads_out.at[other], heads_in.at[tp], heads_send, heads_recv, sp, other
        ).start()
    heads_in[tp] = heads_out[tp]

    for load in loads:
        load.wait()

    settle(heads_in.at[pl.ds(0, 15)], heads_recv)
    low_lane = lax.broadcasted_iota(jnp.int32, (16, 128), 1) < 64
    tokens = jnp.concatenate(
        [
            jnp.where(
                low_lane,
                heads_in[2 * i].astype(jnp.float32),
                heads_in[2 * i + 1].astype(jnp.float32),
            ).astype(jnp.bfloat16)
            for i in range(8)
        ],
        axis=1,
    )
    mixed_f = (
        (residual_ref[...].astype(jnp.float32) + dot_f32(tokens, mix_mat[...]))
        .astype(jnp.bfloat16)
        .astype(jnp.float32)
    )
    mixed_ref[...] = mixed_f
    normed = (
        mixed_f
        * lax.rsqrt(jnp.mean(mixed_f * mixed_f, axis=1, keepdims=True) + norm_eps)
        * norm_ref[...]
    ).astype(jnp.bfloat16)
    stacked = jnp.concatenate([normed[:, q * 512 : (q + 1) * 512] for q in range(4)], axis=0)
    outgoing[...] = dot_f32(spread, stacked).astype(jnp.bfloat16).reshape(16, 16, 512)
    row_at, col_at = sp // 4, sp % 4

    def spread_copy(source, target, at):
        return transfer(
            outgoing.at[target], incoming.at[source], spread_send, spread_recv.at[at], target, tp
        )

    for i in range(4):
        for k in range(4):
            if i == 0 and k == 0:
                continue
            other = ((row_at + 4 - i) % 4) * 4 + (col_at + k) % 4
            spread_copy(sp, other, i).start()
    incoming[sp] = outgoing[sp]

    noted = heads_in[...].astype(jnp.float32)
    every = jnp.concatenate(
        [noted[t][:, (1 - t % 2) * 64 : (1 - t % 2) * 64 + 8] for t in range(16)], axis=0
    )
    score_0 = every[:, 2:3] + every[:, 3:4] + every[:, 4:5]
    score_1 = every[:, 5:6] + every[:, 6:7] + every[:, 7:8]
    rank_0, rank_1 = ranks_of(every[:, 0:1], every[:, 1:2])
    gap = score_1 - score_0
    wide_lane = lax.broadcasted_iota(jnp.int32, (256, 128), 1)
    kept = jnp.zeros((256, 128), jnp.float32)
    for at, column in enumerate(
        (
            every[:, 0:1] * 16.0 + rank_0,
            every[:, 1:2] * 16.0 + rank_1,
            1.0 / (1.0 + jnp.exp(gap)),
            1.0 / (1.0 + jnp.exp(-gap)),
            every[:, 0:1] * 8.0 + rank_0,
            every[:, 1:2] * 8.0 + rank_1,
        )
    ):
        kept = jnp.where(wide_lane == at, column, kept)
    codes[...] = kept.reshape(16, 16, 128)

    following = (((level + 1) % 8) * 2 + core, ((level + 7) % 8) * 2 + core)

    def block_at(distance, way):
        if way == 0:
            return (level + 8 - distance) % 8
        return (level + distance) % 8

    def turn(sub):
        return (row_at + sub) % 4

    def piece_of(index, sub):
        return rows_all.at[index, pl.ds(pl.multiple_of(turn(sub) * sub_rows, sub_rows), sub_rows)]

    def arrival(distance, sub, way):
        return (distance - 1) * subs + sub if distance < 4 else 3 * subs + sub % 2

    def travels(distance, sub, way):
        return distance < 4 or (sub < 2) == (way == 0)

    def ring(index, sub, distance, way):
        slot = arrival(distance, sub, way)
        return transfer(
            piece_of(index, sub),
            piece_of(index, sub),
            ring_send,
            ring_recv.at[way, slot],
            sp,
            following[way],
        )

    def twinned(index, sub, distance):
        return transfer(
            piece_of(index, sub), piece_of(index, sub), twin_send, twin_recv.at[distance], sp, twin
        )

    small_row = lax.broadcasted_iota(jnp.int32, (64, 64), 0)
    small_col = lax.broadcasted_iota(jnp.int32, (64, 64), 1)
    regroup = jnp.where(
        small_col == ((small_row >> 2) & 3) * 16 + (small_row >> 4) * 4 + (small_row & 3), 1.0, 0.0
    ).astype(jnp.bfloat16)
    for sub in range(subs):
        settle(incoming.at[pl.ds(0, 3 if sub == 0 else 4)], spread_recv.at[sub])
        regrouped = dot_f32(
            regroup, incoming[pl.ds(turn(sub) * 4, 4)].reshape(64, 512)
        ).astype(jnp.bfloat16)
        rows_all[tp, pl.ds(pl.multiple_of(turn(sub) * sub_rows, sub_rows), sub_rows)] = (
            jnp.concatenate([regrouped[q * 16 : (q + 1) * 16] for q in range(4)], axis=1)
        )
        for way in (0, 1):
            ring(tp, sub, 1, way).start()
        twinned(tp, sub, 0).start()

    def forward(distance, sub):
        for way in (0, 1):
            if not travels(distance, sub, way):
                continue
            index = block_at(distance, way) * 2 + core
            ring(index, sub, distance, way).wait_recv()
            if distance < 4 and travels(distance + 1, sub, way):
                ring(index, sub, distance + 1, way).start()
            twinned(index, sub, distance).start()

    def await_twin(distance):
        settle(rows_all.at[pl.ds(0, 1 if distance in (0, 4) else 2)], twin_recv.at[distance])

    def members(distance):
        low = block_at(distance, 0) * 2
        if distance in (0, 4):
            return (low, low + 1)
        high = block_at(distance, 1) * 2
        return (low, low + 1, high, high + 1)

    def buffers(distance):
        if distance in (0, 4):
            at = distance // 4
            return (
                pair_out_s.at[at],
                pair_in_s.at[at],
                leave_s.at[at],
                back_s.at[at],
                sent_sum_s.at[at],
            )
        at = distance - 1
        return pair_out.at[at], pair_in.at[at], leave.at[at], back.at[at], sent_sum.at[at]

    def order_of(parts):
        count = parts * 64
        row = lax.broadcasted_iota(jnp.int32, (count, count), 0)
        col = lax.broadcasted_iota(jnp.int32, (count, count), 1)
        source = ((row >> 2) & (parts - 1)) * 64 + (row // (4 * parts)) * 4 + (row & 3)
        return jnp.where(col == source, 1.0, 0.0).astype(jnp.bfloat16)

    reorder = {2: order_of(2), 4: order_of(4)}
    core_at = pl.multiple_of(core * half, half)
    twin_at = pl.multiple_of((1 - core) * half, half)
    across = (((1,), (1,)), ((), ()))

    gate_nat[...] = jnp.transpose(gate_mat[...])
    up_nat[...] = jnp.transpose(up_mat[...])

    def rows_in(distance):
        return jnp.concatenate([rows_all[index] for index in members(distance)], axis=0)

    def stage_gate(distance):
        count = 64 * len(members(distance))
        gate_act[:count] = dot_f32(rows_in(distance), gate_nat[...])

    def stage_up(distance):
        parts = len(members(distance))
        up_act = dot_f32(rows_in(distance), up_nat[...])
        gate = gate_act[: 64 * parts]
        hidden = (gate / (1.0 + jnp.exp(-gate)) * up_act).astype(jnp.bfloat16)
        hidden_rows[: 64 * parts] = dot_f32(reorder[parts], hidden).astype(jnp.bfloat16)

    def pair(distance):
        out, arrived = buffers(distance)[:2]
        return transfer(out, arrived, pair_send.at[distance], pair_recv.at[distance], sp, twin)

    def stage_other(distance):
        count = 64 * len(members(distance))
        buffers(distance)[0][...] = dot_f32(
            hidden_rows[:count], down_mat[:, pl.ds(twin_at, half)]
        ).astype(jnp.bfloat16)
        pair(distance).start()

    def stage_mine(distance):
        count = 64 * len(members(distance))
        mine_part[:count] = dot_f32(hidden_rows[:count], down_mat[:, pl.ds(core_at, half)])

    def back_copy(distance, source, target):
        _, _, out, arrived, _ = buffers(distance)
        return transfer(
            out.at[target],
            arrived.at[source],
            back_send.at[distance],
            back_recv.at[distance],
            target,
            tp,
        )

    def stage_return(distance):
        parts = len(members(distance))
        _, arrived, out, home, _ = buffers(distance)
        pair(distance).wait_recv()
        out[...] = (
            (mine_part[: 64 * parts] + arrived[...].astype(jnp.float32))
            .reshape(16, 4 * parts, half)
            .astype(jnp.bfloat16)
        )
        for j in range(1, 16):
            back_copy(distance, sp, (sp + j) % 16).start()
        home[sp] = out[sp]

    def stage_combine(distance):
        parts = len(members(distance))
        _, _, _, home, leaving = buffers(distance)
        settle(home.at[pl.ds(0, 15)], back_recv.at[distance])
        column = 0 if parts == 4 else 4
        columns = 64 * parts
        lanes = lax.broadcasted_iota(jnp.int32, (16, columns), 1).astype(jnp.float32)
        weights = []
        for place_in, index in enumerate(members(distance)):
            code = codes[index]
            first_at = code[:, column : column + 1] + 4.0 * place_in
            second_at = code[:, column + 1 : column + 2] + 4.0 * place_in
            weights.append(
                jnp.where(lanes == first_at, code[:, 2:3], 0.0)
                + jnp.where(lanes == second_at, code[:, 3:4], 0.0)
            )
        top, low = split_two(jnp.concatenate(weights, axis=0))
        returned = (
            home[...].astype(jnp.float32).reshape(columns, half).astype(jnp.bfloat16)
            if parts == 2
            else home[...].reshape(columns, half)
        )
        leaving[...] = (
            (dot_f32(top, returned) + dot_f32(low, returned)).astype(jnp.bfloat16).reshape(parts, 16, half)
        )

        def send(place_in, index):
            transfer(leaving.at[place_in], got_sum.at[tp], sum_send, sum_recv, sp, index).start()

        if distance == 0:
            send(1 - core, twin)
            got_sum[tp] = leaving[core]
        else:
            for place_in, index in enumerate(members(distance)):
                send(place_in, index)

    for distance in (0, 1, 2, 3):
        await_twin(distance)
        stage_gate(distance)
        forward(distance + 1, 0)
        stage_up(distance)
        forward(distance + 1, 1)
        stage_other(distance)
        forward(distance + 1, 2)
        stage_mine(distance)
        forward(distance + 1, 3)
        stage_return(distance)
        if distance > 0:
            stage_combine(distance - 1)
    await_twin(4)
    stage_gate(4)
    stage_up(4)
    stage_other(4)
    stage_mine(4)
    stage_return(4)
    stage_combine(3)
    stage_combine(4)

    settle(got_sum.at[pl.ds(0, 15)], sum_recv)
    for side in (0, 1):
        gathered = got_sum[side].astype(jnp.float32)
        for stage in range(1, 8):
            gathered = gathered + got_sum[2 * stage + side].astype(jnp.float32)
        cut = slice(side * half, (side + 1) * half)
        out_ref[:, cut] = mixed_ref[:, cut] + gathered
    settle(heads_out.at[pl.ds(0, 15)], heads_send)
    settle(outgoing.at[pl.ds(0, 15)], spread_send)
    settle(rows_all.at[pl.ds(0, 7)], ring_send)
    settle(rows_all.at[pl.ds(0, 8)], twin_send)
    settle(got_sum.at[pl.ds(0, 15)], sum_send)
    for distance in range(5):
        pair(distance).wait_send()
        settle(buffers(distance)[2].at[pl.ds(0, 15)], back_send.at[distance])
    for j in range(1, 16):

        @pl.when(sp + j < 16)
        def _():
            state_copy(j, sp, sp + j).wait_send()


def shards(
    receptance,
    key_matrix,
    value_matrix,
    decay_input_term,
    decay_channel_offset,
    head_log_decay,
    context_step_logits,
    head_gate_rows,
    head_norm_scale,
    mixer_output_weight,
    residual,
    expert_norm_scale,
    expert_index_table,
    expert_router_scores,
    expert_gate_weight,
    expert_up_weight,
    expert_down_weight,
):
    vmem = pl.BlockSpec(memory_space=pltpu.VMEM)
    hbm = pl.BlockSpec(memory_space=pl.ANY)
    dma = pltpu.SemaphoreType.DMA
    b16, f32 = jnp.bfloat16, jnp.float32
    total = pl.pallas_call(
        layer_kernel,
        out_shape=jax.ShapeDtypeStruct((16, width), f32),
        in_specs=[vmem] * 13 + [hbm] * 4,
        out_specs=vmem,
        scratch_shapes=[
            pltpu.VMEM((1024, width), b16),
            pltpu.VMEM((448, width), b16),
            pltpu.VMEM((448, width), b16),
            pltpu.VMEM((448, width), b16),
            pltpu.VMEM((width, 448), b16),
            pltpu.VMEM((width, 448), b16),
            pltpu.VMEM((seq_len, 64), f32),
            pltpu.VMEM((seq_len, 64), f32),
            pltpu.VMEM((64, 128), b16),
            pltpu.VMEM((16, 64, 128), b16),
            pltpu.VMEM((16, 16, 128), b16),
            pltpu.VMEM((16, 16, 128), b16),
            pltpu.VMEM((16, width), f32),
            pltpu.VMEM((16, 4), f32),
            pltpu.VMEM((16, 16, 512), b16),
            pltpu.VMEM((16, 16, 512), b16),
            pltpu.VMEM((16, 16, 128), f32),
            pltpu.VMEM((16, 64, width), b16),
            pltpu.VMEM((256, 448), f32),
            pltpu.VMEM((256, 448), b16),
            pltpu.VMEM((256, half), f32),
            pltpu.VMEM((3, 256, half), b16),
            pltpu.VMEM((3, 256, half), b16),
            pltpu.VMEM((3, 16, 16, half), b16),
            pltpu.VMEM((3, 16, 16, half), b16),
            pltpu.VMEM((3, 4, 16, half), b16),
            pltpu.VMEM((2, 128, half), b16),
            pltpu.VMEM((2, 128, half), b16),
            pltpu.VMEM((2, 16, 8, half), b16),
            pltpu.VMEM((2, 16, 8, half), b16),
            pltpu.VMEM((2, 2, 16, half), b16),
            pltpu.VMEM((16, 16, half), b16),
            dma((4,)),
            dma((16,)),
            dma((16,)),
            dma((7,)),
            dma((4,)),
            dma((2, 14)),
        ]
        + [dma((5,))] * 5,
        compiler_params=pltpu.CompilerParams(
            collective_id=1, has_side_effects=True, vmem_limit_bytes=56 * 1024 * 1024
        ),
    )(
        receptance.T,
        key_matrix.T,
        value_matrix.T,
        decay_input_term.T,
        decay_channel_offset.reshape(1, -1),
        head_log_decay.T,
        context_step_logits.T,
        head_gate_rows.T,
        head_norm_scale.reshape(1, -1),
        residual,
        expert_norm_scale.reshape(1, -1),
        expert_index_table.T,
        expert_router_scores.T,
        mixer_output_weight,
        jnp.swapaxes(expert_gate_weight, 1, 2),
        jnp.swapaxes(expert_up_weight, 1, 2),
        expert_down_weight,
    )
    return total.astype(b16)


def solution(mesh):
    return jax.shard_map(
        shards,
        mesh=mesh,
        in_specs=(
            P("sp", "tp"),
            P("sp", "tp"),
            P("sp", "tp"),
            P("sp", "tp"),
            P("tp"),
            P("sp", "tp"),
            P("sp", "tp"),
            P("sp", "tp"),
            P("tp"),
            P(),
            P(("sp", "tp"), None),
            P(),
            P(("sp", "tp"), None),
            P(("sp", "tp"), None),
            P("sp", None, "tp"),
            P("sp", None, "tp"),
            P("sp", "tp", None),
        ),
        out_specs=P(("sp", "tp"), None),
        check_vma=False,
    )
```

time: 86.9 us -> 80.3 us (0.924)
  Pallas kernels: 85.3 us -> 78.6 us
  other arithmetic: 0 us -> 1.54 us
  local copies, waits for them, and re-layouts: 1.47 us -> 0 us
    pallas_call x1, Pallas kernels: 85.3 us -> 78.6 us  [shards(): pl.pallas_call(layer_kernel, out_shape=jax.ShapeDtypeStruct((16, width),...]
    convert_element_type x0 -> x1, other arithmetic: none -> 1.54 us  [shards(): return total.astype(b16)]
    unnamed x1 -> x0, local copies, waits for them, and re-layouts: 1.47 us -> none
where the time goes in v3:
time: 80.3 us; the launch traced here: 80.2 us
  Pallas kernels  78.6 us (98%)
  other arithmetic  1.54 us (2%)
    pallas_call x1, Pallas kernels, shards(): pl.pallas_call(layer_kernel, out_shape=jax.ShapeDtypeStruct((16, width),...  78.6 us

profile of v3, /device:TPU:1, one launch (start us, length us, event | category | flops | bytes accessed | tf_op | source)
XLA Modules:
  0.0 80.2 jit_solution(16237450699332624931)
XLA Ops:
  0.0 78.6 %shard_map.163 = f32[16,2048]{1,0:T(8,128)} custom-call(bf16[64,256]{1,0:T(8,128)(2,1)} %bitcast.16, bf16[64,256]{1,0:T(8,128)(2,1)} %bitcast.17, bf16[64,256]{1,0:T(8,128)(2,1)} %bitcast.18, bf16[64,256]{1,0:T(8,128)(2,1)} %bitcast.19, f32[1,64]{1,0:T(1,128)} %bitcast.26, f32[1,256]{1,0:T(1,128)} %bitcast.23, bf16[64,256]{1,0:T(8,128)(2,1)} %bitcast.20, ...), custom_call_target="tpu_custom_call" | custom-call | tf_op jit(solution)/shard_map/pallas_call | solution.py:730
  78.6 1.5 %convert_element_type.3 = bf16[16,2048]{1,0:T(8,128)(2,1)} convert(f32[16,2048]{1,0:T(8,128)} %shard_map.163) | non-fusion elementwise | flops 32768 | bytes 196608 | tf_op jit(solution)/shard_map/convert_element_type | solution.py:798

commit v4 on v3

--- a/solution.py
+++ b/solution.py
@@ -272,6 +272,10 @@
     table_ref,
     outgoing,
     incoming,
+    raw_out,
+    raw_in,
+    far_out,
+    far_in,
     codes,
     rows_all,
     gate_act,
@@ -303,9 +307,20 @@
     sp, tp = lax.axis_index("sp"), lax.axis_index("tp")
     level, core = tp // 2, tp % 2
     twin = level * 2 + (1 - core)
-    heads_send, heads_recv, spread_send, ring_send, twin_send, sum_send, sum_recv = (
-        single_sem.at[k] for k in range(7)
-    )
+    opposite = (tp + 8) % 16
+    (
+        heads_send,
+        heads_recv,
+        spread_send,
+        ring_send,
+        twin_send,
+        sum_send,
+        sum_recv,
+        raw_send,
+        raw_recv,
+        far_send,
+        far_recv,
+    ) = (single_sem.at[k] for k in range(11))
 
     loads = [
         pltpu.make_async_copy(source, target, weight_sem.at[k])
@@ -362,17 +377,24 @@
 
     own_table = table_ref[...]
     rank_0, rank_1 = ranks_of(own_table[:, 0:1], own_table[:, 1:2])
-    first, second = own_table[:, 0:1] * 16.0 + rank_0, own_table[:, 1:2] * 16.0 + rank_1
-    lane = lax.broadcasted_iota(jnp.int32, (16, 256), 1).astype(jnp.float32)
-    spread = jnp.transpose(
-        jnp.concatenate(
-            [
-                jnp.where((lane == first + 4.0 * q) | (lane == second + 4.0 * q), 1.0, 0.0)
-                for q in range(4)
-            ],
-            axis=0,
-        )
-    ).astype(jnp.bfloat16)
+
+    def spread_of(first, second):
+        lane = lax.broadcasted_iota(jnp.int32, (16, 256), 1).astype(jnp.float32)
+        return jnp.transpose(
+            jnp.concatenate(
+                [
+                    jnp.where((lane == first + 4.0 * q) | (lane == second + 4.0 * q), 1.0, 0.0)
+                    for q in range(4)
+                ],
+                axis=0,
+            )
+        ).astype(jnp.bfloat16)
+
+    def spread_rows(spread, rows):
+        stacked = jnp.concatenate([rows[:, q * 512 : (q + 1) * 512] for q in range(4)], axis=0)
+        return dot_f32(spread, stacked).astype(jnp.bfloat16).reshape(16, 16, 512)
+
+    spread = spread_of(own_table[:, 0:1] * 16.0 + rank_0, own_table[:, 1:2] * 16.0 + rank_1)
 
     for j in range(1, 16):
 
@@ -406,6 +428,7 @@
 
     for load in loads:
         load.wait()
+    gate_nat[...] = jnp.transpose(gate_mat[...])
 
     settle(heads_in.at[pl.ds(0, 15)], heads_recv)
     low_lane = lax.broadcasted_iota(jnp.int32, (16, 128), 1) < 64
@@ -431,8 +454,10 @@
         * lax.rsqrt(jnp.mean(mixed_f * mixed_f, axis=1, keepdims=True) + norm_eps)
         * norm_ref[...]
     ).astype(jnp.bfloat16)
-    stacked = jnp.concatenate([normed[:, q * 512 : (q + 1) * 512] for q in range(4)], axis=0)
-    outgoing[...] = dot_f32(spread, stacked).astype(jnp.bfloat16).reshape(16, 16, 512)
+    raw_out[...] = normed
+    raw_copy = transfer(raw_out, raw_in, raw_send, raw_recv, sp, opposite)
+    raw_copy.start()
+    outgoing[...] = spread_rows(spread, normed)
     row_at, col_at = sp // 4, sp % 4
 
     def spread_copy(source, target, at):
@@ -470,6 +495,7 @@
     ):
         kept = jnp.where(wide_lane == at, column, kept)
     codes[...] = kept.reshape(16, 16, 128)
+    up_nat[...] = jnp.transpose(up_mat[...])
 
     following = (((level + 1) % 8) * 2 + core, ((level + 7) % 8) * 2 + core)
 
@@ -484,14 +510,11 @@
     def piece_of(index, sub):
         return rows_all.at[index, pl.ds(pl.multiple_of(turn(sub) * sub_rows, sub_rows), sub_rows)]
 
-    def arrival(distance, sub, way):
-        return (distance - 1) * subs + sub if distance < 4 else 3 * subs + sub % 2
-
-    def travels(distance, sub, way):
-        return distance < 4 or (sub < 2) == (way == 0)
+    def arrival(distance, sub):
+        return (distance - 1) * subs + sub
 
     def ring(index, sub, distance, way):
-        slot = arrival(distance, sub, way)
+        slot = arrival(distance, sub)
         return transfer(
             piece_of(index, sub),
             piece_of(index, sub),
@@ -501,9 +524,9 @@
             following[way],
         )
 
-    def twinned(index, sub, distance):
+    def twinned(index, sub, piece):
         return transfer(
-            piece_of(index, sub), piece_of(index, sub), twin_send, twin_recv.at[distance], sp, twin
+            piece_of(index, sub), piece_of(index, sub), twin_send, twin_recv.at[piece], sp, twin
         )
 
     small_row = lax.broadcasted_iota(jnp.int32, (64, 64), 0)
@@ -523,29 +546,48 @@
             ring(tp, sub, 1, way).start()
         twinned(tp, sub, 0).start()
 
+    raw_copy.wait_recv()
+    far_codes = codes[opposite]
+    far_out[...] = spread_rows(spread_of(far_codes[:, 0:1], far_codes[:, 1:2]), raw_in[...])
+    for j in range(1, 16):
+        other = (sp + j) % 16
+        transfer(far_out.at[other], far_in.at[sp], far_send, far_recv, other, tp).start()
+    far_in[sp] = far_out[sp]
+
+    def far_arrives():
+        settle(far_in.at[pl.ds(0, 15)], far_recv)
+        for sub in range(subs):
+            regrouped = dot_f32(
+                regroup, far_in[sub * 4 : (sub + 1) * 4].reshape(64, 512)
+            ).astype(jnp.bfloat16)
+            rows_all[opposite, sub * sub_rows : (sub + 1) * sub_rows] = jnp.concatenate(
+                [regrouped[q * 16 : (q + 1) * 16] for q in range(4)], axis=1
+            )
+        transfer(
+            rows_all.at[opposite], rows_all.at[opposite], twin_send, twin_recv.at[4], sp, twin
+        ).start()
+
     def forward(distance, sub):
         for way in (0, 1):
-            if not travels(distance, sub, way):
-                continue
             index = block_at(distance, way) * 2 + core
             ring(index, sub, distance, way).wait_recv()
-            if distance < 4 and travels(distance + 1, sub, way):
+            if distance < 3:
                 ring(index, sub, distance + 1, way).start()
-            twinned(index, sub, distance).start()
+            twinned(index, sub, 5 if distance == 3 and way == 1 else distance).start()
 
     def await_twin(distance):
-        settle(rows_all.at[pl.ds(0, 1 if distance in (0, 4) else 2)], twin_recv.at[distance])
+        settle(rows_all.at[pl.ds(0, 2 if distance in (1, 2) else 1)], twin_recv.at[distance])
 
     def members(distance):
-        low = block_at(distance, 0) * 2
-        if distance in (0, 4):
+        low = block_at(3, 1) * 2 if distance == 5 else block_at(distance, 0) * 2
+        if distance not in (1, 2):
             return (low, low + 1)
         high = block_at(distance, 1) * 2
         return (low, low + 1, high, high + 1)
 
     def buffers(distance):
-        if distance in (0, 4):
-            at = distance // 4
+        if distance not in (1, 2):
+            at = (0, None, None, 2, 1, 3)[distance]
             return (
                 pair_out_s.at[at],
                 pair_in_s.at[at],
@@ -567,9 +609,6 @@
     core_at = pl.multiple_of(core * half, half)
     twin_at = pl.multiple_of((1 - core) * half, half)
     across = (((1,), (1,)), ((), ()))
-
-    gate_nat[...] = jnp.transpose(gate_mat[...])
-    up_nat[...] = jnp.transpose(up_mat[...])
 
     def rows_in(distance):
         return jnp.concatenate([rows_all[index] for index in members(distance)], axis=0)
@@ -660,27 +699,52 @@
             for place_in, index in enumerate(members(distance)):
                 send(place_in, index)
 
-    for distance in (0, 1, 2, 3):
+    def stages_up(distance):
         await_twin(distance)
         stage_gate(distance)
-        forward(distance + 1, 0)
         stage_up(distance)
-        forward(distance + 1, 1)
+
+    def stages_down(distance):
         stage_other(distance)
-        forward(distance + 1, 2)
         stage_mine(distance)
-        forward(distance + 1, 3)
-        stage_return(distance)
-        if distance > 0:
-            stage_combine(distance - 1)
-    await_twin(4)
-    stage_gate(4)
-    stage_up(4)
-    stage_other(4)
-    stage_mine(4)
+
+    stages_up(0)
+    forward(1, 0)
+    stages_down(0)
+    forward(1, 1)
+    stage_return(0)
+    forward(1, 2)
+    forward(1, 3)
+    stages_up(1)
+    forward(2, 0)
+    stages_down(1)
+    far_arrives()
+    forward(2, 1)
+    stage_return(1)
+    forward(2, 2)
+    stages_up(4)
+    stages_down(4)
+    forward(2, 3)
     stage_return(4)
+    stages_up(2)
+    forward(3, 0)
+    stages_down(2)
+    forward(3, 1)
+    stage_return(2)
+    forward(3, 2)
+    stage_combine(0)
+    forward(3, 3)
+    stages_up(3)
+    stages_down(3)
+    stages_up(5)
+    stage_return(3)
+    stages_down(5)
+    stage_return(5)
+    stage_combine(1)
+    stage_combine(4)
+    stage_combine(2)
     stage_combine(3)
-    stage_combine(4)
+    stage_combine(5)
 
     settle(got_sum.at[pl.ds(0, 15)], sum_recv)
     for side in (0, 1):
@@ -691,10 +755,12 @@
         out_ref[:, cut] = mixed_ref[:, cut] + gathered
     settle(heads_out.at[pl.ds(0, 15)], heads_send)
     settle(outgoing.at[pl.ds(0, 15)], spread_send)
-    settle(rows_all.at[pl.ds(0, 7)], ring_send)
+    settle(rows_all.at[pl.ds(0, 6)], ring_send)
+    settle(raw_out, raw_send)
+    settle(far_out.at[pl.ds(0, 15)], far_send)
     settle(rows_all.at[pl.ds(0, 8)], twin_send)
     settle(got_sum.at[pl.ds(0, 15)], sum_send)
-    for distance in range(5):
+    for distance in range(6):
         pair(distance).wait_send()
         settle(buffers(distance)[2].at[pl.ds(0, 15)], back_send.at[distance])
     for j in range(1, 16):
@@ -749,30 +815,34 @@
             pltpu.VMEM((16, 4), f32),
             pltpu.VMEM((16, 16, 512), b16),
             pltpu.VMEM((16, 16, 512), b16),
+            pltpu.VMEM((16, width), b16),
+            pltpu.VMEM((16, width), b16),
+            pltpu.VMEM((16, 16, 512), b16),
+            pltpu.VMEM((16, 16, 512), b16),
             pltpu.VMEM((16, 16, 128), f32),
             pltpu.VMEM((16, 64, width), b16),
             pltpu.VMEM((256, 448), f32),
             pltpu.VMEM((256, 448), b16),
             pltpu.VMEM((256, half), f32),
-            pltpu.VMEM((3, 256, half), b16),
-            pltpu.VMEM((3, 256, half), b16),
-            pltpu.VMEM((3, 16, 16, half), b16),
-            pltpu.VMEM((3, 16, 16, half), b16),
-            pltpu.VMEM((3, 4, 16, half), b16),
-            pltpu.VMEM((2, 128, half), b16),
-            pltpu.VMEM((2, 128, half), b16),
-            pltpu.VMEM((2, 16, 8, half), b16),
-            pltpu.VMEM((2, 16, 8, half), b16),
-            pltpu.VMEM((2, 2, 16, half), b16),
+            pltpu.VMEM((2, 256, half), b16),
+            pltpu.VMEM((2, 256, half), b16),
+            pltpu.VMEM((2, 16, 16, half), b16),
+            pltpu.VMEM((2, 16, 16, half), b16),
+            pltpu.VMEM((2, 4, 16, half), b16),
+            pltpu.VMEM((4, 128, half), b16),
+            pltpu.VMEM((4, 128, half), b16),
+            pltpu.VMEM((4, 16, 8, half), b16),
+            pltpu.VMEM((4, 16, 8, half), b16),
+            pltpu.VMEM((4, 2, 16, half), b16),
             pltpu.VMEM((16, 16, half), b16),
             dma((4,)),
             dma((16,)),
             dma((16,)),
-            dma((7,)),
+            dma((11,)),
             dma((4,)),
-            dma((2, 14)),
+            dma((2, 12)),
         ]
-        + [dma((5,))] * 5,
+        + [dma((6,))] * 5,
         compiler_params=pltpu.CompilerParams(
             collective_id=1, has_side_effects=True, vmem_limit_bytes=56 * 1024 * 1024
         ),

time: 80.3 us -> 73.6 us (0.917)
  Pallas kernels: 78.6 us -> 71.9 us
    pallas_call x1, Pallas kernels: 78.6 us -> 71.9 us  [shards(): pl.pallas_call(layer_kernel, out_shape=jax.ShapeDtypeStruct((16, width),...]
where the time goes in v4:
time: 73.6 us; the launch traced here: 73.4 us
  Pallas kernels  71.9 us (98%)
  other arithmetic  1.54 us (2%)
    pallas_call x1, Pallas kernels, shards(): pl.pallas_call(layer_kernel, out_shape=jax.ShapeDtypeStruct((16, width),...  71.9 us
    convert_element_type x1, other arithmetic, shards(): return total.astype(b16)  1.54 us

profile of v4, /device:TPU:1, one launch (start us, length us, event | category | flops | bytes accessed | tf_op | source)
XLA Modules:
  0.0 73.4 jit_solution(8083092714302466770)
XLA Ops:
  0.0 71.9 %shard_map.163 = f32[16,2048]{1,0:T(8,128)} custom-call(bf16[64,256]{1,0:T(8,128)(2,1)} %bitcast.16, bf16[64,256]{1,0:T(8,128)(2,1)} %bitcast.17, bf16[64,256]{1,0:T(8,128)(2,1)} %bitcast.18, bf16[64,256]{1,0:T(8,128)(2,1)} %bitcast.19, f32[1,64]{1,0:T(1,128)} %bitcast.26, f32[1,256]{1,0:T(1,128)} %bitcast.23, bf16[64,256]{1,0:T(8,128)(2,1)} %bitcast.20, ...), custom_call_target="tpu_custom_call" | custom-call | tf_op jit(solution)/shard_map/pallas_call | solution.py:796
  71.9 1.5 %convert_element_type.3 = bf16[16,2048]{1,0:T(8,128)(2,1)} convert(f32[16,2048]{1,0:T(8,128)} %shard_map.163) | non-fusion elementwise | flops 32768 | bytes 196608 | tf_op jit(solution)/shard_map/convert_element_type | solution.py:868

commit v5 on v4

--- a/solution.py
+++ b/solution.py
@@ -573,20 +573,27 @@
             ring(index, sub, distance, way).wait_recv()
             if distance < 3:
                 ring(index, sub, distance + 1, way).start()
-            twinned(index, sub, 5 if distance == 3 and way == 1 else distance).start()
+            piece = distance
+            if distance == 3 and way == 1:
+                piece = 5
+            if distance == 1 and sub > 1:
+                piece = 6
+            twinned(index, sub, piece).start()
 
     def await_twin(distance):
-        settle(rows_all.at[pl.ds(0, 2 if distance in (1, 2) else 1)], twin_recv.at[distance])
+        settle(rows_all.at[pl.ds(0, 2 if distance == 2 else 1)], twin_recv.at[distance])
 
     def members(distance):
+        if distance == 6:
+            distance = 1
         low = block_at(3, 1) * 2 if distance == 5 else block_at(distance, 0) * 2
-        if distance not in (1, 2):
+        if distance not in (1, 2, 6):
             return (low, low + 1)
         high = block_at(distance, 1) * 2
         return (low, low + 1, high, high + 1)
 
     def buffers(distance):
-        if distance not in (1, 2):
+        if distance not in (1, 2, 6):
             at = (0, None, None, 2, 1, 3)[distance]
             return (
                 pair_out_s.at[at],
@@ -595,7 +602,7 @@
                 back_s.at[at],
                 sent_sum_s.at[at],
             )
-        at = distance - 1
+        at = 1 if distance == 2 else 0
         return pair_out.at[at], pair_in.at[at], leave.at[at], back.at[at], sent_sum.at[at]
 
     def order_of(parts):
@@ -606,37 +613,60 @@
         return jnp.where(col == source, 1.0, 0.0).astype(jnp.bfloat16)
 
     reorder = {2: order_of(2), 4: order_of(4)}
+    half_row = lax.broadcasted_iota(jnp.int32, (128, 128), 0)
+    half_col = lax.broadcasted_iota(jnp.int32, (128, 128), 1)
+    half_order = jnp.where(
+        half_col == ((half_row >> 2) & 3) * 32 + (half_row >> 4) * 4 + (half_row & 3), 1.0, 0.0
+    ).astype(jnp.bfloat16)
+
+    def part_of(distance):
+        return pl.ds(128 if distance == 6 else 0, 256 if distance == 2 else 128)
     core_at = pl.multiple_of(core * half, half)
     twin_at = pl.multiple_of((1 - core) * half, half)
     across = (((1,), (1,)), ((), ()))
 
     def rows_in(distance):
+        if distance in (1, 6):
+            first = 0 if distance == 1 else 2
+            return jnp.concatenate(
+                [
+                    piece_of(index, first + i)[...]
+                    for index in members(distance)
+                    for i in range(2)
+                ],
+                axis=0,
+            )
         return jnp.concatenate([rows_all[index] for index in members(distance)], axis=0)
 
+    def count_of(distance):
+        return 256 if distance == 2 else 128
+
     def stage_gate(distance):
-        count = 64 * len(members(distance))
+        count = count_of(distance)
         gate_act[:count] = dot_f32(rows_in(distance), gate_nat[...])
 
     def stage_up(distance):
-        parts = len(members(distance))
+        count = count_of(distance)
+        order = half_order if distance in (1, 6) else reorder[count // 64]
         up_act = dot_f32(rows_in(distance), up_nat[...])
-        gate = gate_act[: 64 * parts]
+        gate = gate_act[:count]
         hidden = (gate / (1.0 + jnp.exp(-gate)) * up_act).astype(jnp.bfloat16)
-        hidden_rows[: 64 * parts] = dot_f32(reorder[parts], hidden).astype(jnp.bfloat16)
+        hidden_rows[:count] = dot_f32(order, hidden).astype(jnp.bfloat16)
 
     def pair(distance):
         out, arrived = buffers(distance)[:2]
+        out, arrived = out.at[part_of(distance)], arrived.at[part_of(distance)]
         return transfer(out, arrived, pair_send.at[distance], pair_recv.at[distance], sp, twin)
 
     def stage_other(distance):
-        count = 64 * len(members(distance))
-        buffers(distance)[0][...] = dot_f32(
+        count = count_of(distance)
+        buffers(distance)[0][part_of(distance)] = dot_f32(
             hidden_rows[:count], down_mat[:, pl.ds(twin_at, half)]
         ).astype(jnp.bfloat16)
         pair(distance).start()
 
     def stage_mine(distance):
-        count = 64 * len(members(distance))
+        count = count_of(distance)
         mine_part[:count] = dot_f32(hidden_rows[:count], down_mat[:, pl.ds(core_at, half)])
 
     def back_copy(distance, source, target):
@@ -644,8 +674,8 @@
         return transfer(
             out.at[target],
             arrived.at[source],
-            back_send.at[distance],
-            back_recv.at[distance],
+            back_send.at[1 if distance == 6 else distance],
+            back_recv.at[1 if distance == 6 else distance],
             target,
             tp,
         )
@@ -654,6 +684,24 @@
         parts = len(members(distance))
         _, arrived, out, home, _ = buffers(distance)
         pair(distance).wait_recv()
+        if distance in (1, 6):
+            summed = (
+                (mine_part[:128] + arrived[part_of(distance)].astype(jnp.float32))
+                .astype(jnp.bfloat16)
+                .reshape(8, 16, half)
+            )
+            for i in range(2):
+                sub = i + (0 if distance == 1 else 2)
+                out[pl.ds(turn(sub) * 4, 4)] = summed[i * 4 : (i + 1) * 4]
+            for i in range(2):
+                sub = i + (0 if distance == 1 else 2)
+                for k in range(4):
+                    if sub == 0 and k == 0:
+                        continue
+                    back_copy(distance, sp, turn(sub) * 4 + (col_at + k) % 4).start()
+            if distance == 1:
+                home[sp] = out[sp]
+            return
         out[...] = (
             (mine_part[: 64 * parts] + arrived[...].astype(jnp.float32))
             .reshape(16, 4 * parts, half)
@@ -713,14 +761,17 @@
     stages_down(0)
     forward(1, 1)
     stage_return(0)
+    stages_up(1)
     forward(1, 2)
+    stages_down(1)
     forward(1, 3)
-    stages_up(1)
+    stage_return(1)
+    stages_up(6)
     forward(2, 0)
-    stages_down(1)
+    stages_down(6)
     far_arrives()
     forward(2, 1)
-    stage_return(1)
+    stage_return(6)
     forward(2, 2)
     stages_up(4)
     stages_down(4)
@@ -736,12 +787,12 @@
     forward(3, 3)
     stages_up(3)
     stages_down(3)
+    stage_combine(1)
     stages_up(5)
     stage_return(3)
     stages_down(5)
+    stage_combine(4)
     stage_return(5)
-    stage_combine(1)
-    stage_combine(4)
     stage_combine(2)
     stage_combine(3)
     stage_combine(5)
@@ -760,6 +811,7 @@
     settle(far_out.at[pl.ds(0, 15)], far_send)
     settle(rows_all.at[pl.ds(0, 8)], twin_send)
     settle(got_sum.at[pl.ds(0, 15)], sum_send)
+    pair(6).wait_send()
     for distance in range(6):
         pair(distance).wait_send()
         settle(buffers(distance)[2].at[pl.ds(0, 15)], back_send.at[distance])
@@ -842,7 +894,7 @@
             dma((4,)),
             dma((2, 12)),
         ]
-        + [dma((6,))] * 5,
+        + [dma((7,))] * 5,
         compiler_params=pltpu.CompilerParams(
             collective_id=1, has_side_effects=True, vmem_limit_bytes=56 * 1024 * 1024
         ),

time: 73.6 us -> 73.5 us (level)
  no operation moved by 1% of the time
where the time goes in v5:
time: 73.5 us; the launch traced here: 73.4 us
  Pallas kernels  71.9 us (98%)
  other arithmetic  1.54 us (2%)
    pallas_call x1, Pallas kernels, shards(): pl.pallas_call(layer_kernel, out_shape=jax.ShapeDtypeStruct((16, width),...  71.9 us
    convert_element_type x1, other arithmetic, shards(): return total.astype(b16)  1.54 us

profile of v5, /device:TPU:1, one launch (start us, length us, event | category | flops | bytes accessed | tf_op | source)
XLA Modules:
  0.0 73.4 jit_solution(71121173162160634)
XLA Ops:
  0.0 71.9 %shard_map.163 = f32[16,2048]{1,0:T(8,128)} custom-call(bf16[64,256]{1,0:T(8,128)(2,1)} %bitcast.16, bf16[64,256]{1,0:T(8,128)(2,1)} %bitcast.17, bf16[64,256]{1,0:T(8,128)(2,1)} %bitcast.18, bf16[64,256]{1,0:T(8,128)(2,1)} %bitcast.19, f32[1,64]{1,0:T(1,128)} %bitcast.26, f32[1,256]{1,0:T(1,128)} %bitcast.23, bf16[64,256]{1,0:T(8,128)(2,1)} %bitcast.20, ...), custom_call_target="tpu_custom_call" | custom-call | tf_op jit(solution)/shard_map/pallas_call | solution.py:848
  71.9 1.5 %convert_element_type.3 = bf16[16,2048]{1,0:T(8,128)(2,1)} convert(f32[16,2048]{1,0:T(8,128)} %shard_map.163) | non-fusion elementwise | flops 32768 | bytes 196608 | tf_op jit(solution)/shard_map/convert_element_type | solution.py:920
